TPU v7x, 32 devices: a whole 2x2x4 slice. The times are simulated.
32 devices in a mesh: rep: 4 (over z), fs: 4 (over y, x), tp: 2 (over core).
Axes of the slice: x: 2, y: 2, z: 4, core: 2. Of those that a mesh axis runs over, the one named last changes fastest.
Arguments:
- tokens: bfloat16 [8192, 2048], P(('rep', 'fs')), may hold values from -6 to 6
- mix_gain: float32 [2048], replicated, may hold values from 0.1 to 1.9
- w_gate_b: bfloat16 [2048, 1024], P('fs', 'tp'), may hold values from -0.125 to 0.125
- w_gate_c: bfloat16 [2048, 1024], P('fs', 'tp'), may hold values from -0.125 to 0.125
- w_conv_in: bfloat16 [2048, 1024], P('fs', 'tp'), may hold values from -0.125 to 0.125
- conv_taps: float32 [3, 1024], P(None, 'tp'), may hold values from -3 to 3
- w_mix_out: bfloat16 [1024, 2048], P('tp', 'fs'), may hold values from -0.1875 to 0.1875
- ffn_gain: float32 [2048], replicated, may hold values from 0.1 to 1.9
- w_ffn_gate: bfloat16 [2048, 2816], P('fs', 'tp'), may hold values from -0.125 to 0.125
- w_ffn_up: bfloat16 [2048, 2816], P('fs', 'tp'), may hold values from -0.125 to 0.125
- w_ffn_down: bfloat16 [2816, 2048], P('tp', 'fs'), may hold values from -0.109375 to 0.109375
Outputs:
- layer_out: bfloat16 [8192, 2048], P(('rep', 'fs', 'tp'))
All inputs are finite; a program needn't handle non-finite values.
Results may differ from a plain program's by a relative error of at most 0.014.
Values may be sent and summed in bfloat16 or wider, within the bound.
A program may use at most 64 MiB of HBM per device.

v0:
```python
import jax
import jax.numpy as jnp
from jax import lax
from jax.experimental import pallas as pl
from jax.experimental.pallas import tpu as pltpu
from jax.sharding import PartitionSpec as P

LEN = 128
LANES = 128
EPSILON = 1e-06
MESH = pl.DeviceIdType.MESH
F32 = jnp.float32
BF16 = jnp.bfloat16


def rms_scale(values, gain):
    return values * lax.rsqrt(jnp.mean(values * values, axis=-1, keepdims=True) + EPSILON) * gain


N_CHUNKS = 4


def weight_pieces(rows_d, n_conv, n_mix, n_gate_up, n_down, mix_rows, down_rows):
    pieces = [(0, i * rows_d // 2, rows_d // 2, 0, n_conv) for i in range(2)]
    pieces.append((1, 0, mix_rows, 0, n_mix))
    units = n_gate_up // (2 * LANES)
    gate_up = sorted({2 * LANES * u for u in (2 * units // 5, 4 * units // 5, units)} | {0, n_gate_up})
    down = (0, n_down // 2, 3 * n_down // 4, n_down)
    for weight, rows, cuts in ((2, rows_d, gate_up), (3, down_rows, down)):
        pieces += [(weight, 0, rows, a, b - a) for a, b in zip(cuts, cuts[1:])]
    return pieces


def layer_kernel(
    tokens, wb, wc, wi, wm_in, wg_in, wu_in, wd_in, mix_gain_in, taps_in, ffn_gain_in,
    out,
    tok, normed, n2, WA, WM, WG, WD, tile, gated, MP, RS, BR, hidden, OP, RO, ZC, RF, mix_gain, taps, ffn_gain,
    load_sem, ds, dr, fs_, fr, tz_s, tz_r, ts_s, ts_r, g_s, g_r, sib_s, sib_r, z_s, z_r, n_s, n_r,
    o_s, o_r, q_s, q_r,
):
    n_fs, rows_d, _ = WA.shape
    ch = gated.shape[2]
    hid = hidden.shape[1]
    width = tokens.shape[1]
    half = tokens.shape[0] // 4
    cols = WD.shape[2]
    mcols = WM.shape[2]
    full, rest = hid // LANES, hid % LANES

    r = lax.axis_index("rep")
    f = lax.axis_index("fs")
    t = lax.axis_index("tp")
    p = lax.rem(r, 2)
    z_dev = {"rep": r + 1 - 2 * p}
    x_of = f + 1 - 2 * lax.rem(f, 2)
    y_of = lax.rem(f + 2, 4)
    d_of = lax.rem(x_of + 2, 4)
    x_dev, y_dev, s_dev = {"fs": x_of}, {"fs": y_of}, {"tp": 1 - t}

    def part(c, core):
        return pl.ds(pl.multiple_of((2 * c + core) * half, half), half)

    def chunk(c):
        return pl.ds(pl.multiple_of(2 * c * half, 2 * half), 2 * half)

    barrier = pltpu.get_barrier_semaphore()
    for dev in (x_dev, y_dev, z_dev, s_dev):
        pl.semaphore_signal(barrier, inc=1, device_id=dev, device_id_type=MESH)

    chan = pl.ds(pl.multiple_of(p * ch, ch), ch)
    loads = []

    def load(src, dst):
        c = pltpu.make_async_copy(src, dst, load_sem.at[len(loads)])
        c.start()
        loads.append(c)
        return c

    l_wa = []
    for k in range(2):
        rows = pl.ds(k * (rows_d // 2), rows_d // 2)
        l_wa.append([
            load(w.at[rows, chan], WA.at[f, rows, pl.ds(i * ch, ch)]) for i, w in enumerate((wb, wc, wi))
        ])
    l_tok = [
        load(tokens.at[pl.ds((2 * core + h) * half, half)], tok.at[part(2 * h + p, core)])
        for h in range(2) for core in range(2)
    ]
    l_small = [
        load(a, b) for a, b in ((mix_gain_in, mix_gain), (taps_in, taps), (ffn_gain_in, ffn_gain))
    ]
    pl.semaphore_wait(barrier, 4)

    def remote(src, dst, s, rcv, dev):
        return pltpu.make_async_remote_copy(
            src_ref=src, dst_ref=dst, send_sem=s, recv_sem=rcv, device_id=dev, device_id_type=MESH
        )

    bufs = (WA, WM, WG, WD)
    pieces = weight_pieces(rows_d, 3 * ch, mcols, 2 * hid, cols, WM.shape[1], hid)

    def cut(k, slot, first, parts):
        w, r0, n, c0, nc = pieces[k]
        return bufs[w].at[slot, pl.ds(r0 + first * n // 2, parts * n // 2), pl.ds(c0, nc)]

    def direct(k):
        ref = cut(k, f, 0, 2)
        return [remote(ref, ref, ds.at[k, c], dr.at[k, c], dev) for c, dev in ((0, x_dev), (1, y_dev))]

    def forward(k):
        a, b = cut(k, x_of, 0, 1), cut(k, y_of, 1, 1)
        return [
            remote(b, b, fs_.at[k, 0], fr.at[k, 0], x_dev),
            remote(a, a, fs_.at[k, 1], fr.at[k, 1], y_dev),
        ]

    sent = []

    def start(*copies):
        for c in copies:
            c.start()
            sent.append(c)
        return copies

    D, F = {}, {}

    def send(*ks):
        for k in ks:
            D[k] = start(*direct(k))

    def step(k, *more):
        for c in D[k]:
            c.wait_recv()
        F[k] = start(*forward(k))
        send(*more)

    def arrived(*ks):
        for k in ks:
            for c in F[k]:
                c.wait_recv()

    for k in range(2):
        for c in l_wa[k]:
            c.wait()
        send(k)
    for c in l_tok + l_small:
        c.wait()
    tz, ts = [], []
    for h in range(2):
        ref = tok.at[part(2 * h + p, t)]
        tz += start(remote(ref, ref, tz_s.at[h], tz_r.at[h], z_dev))

    def relay(h):
        tz[h].wait_recv()
        ref = tok.at[part(2 * h + 1 - p, t)]
        ts.extend(start(remote(ref, ref, ts_s.at[h], ts_r.at[h], s_dev)))

    def norm_chunk(c):
        def body(i, _):
            rows = pl.ds(pl.multiple_of(2 * c * half + i * 64, 64), 64)
            normed[rows, :] = rms_scale(tok[rows, :].astype(F32), mix_gain[...]).astype(BF16)
            return 0

        lax.fori_loop(0, 2 * half // 64, body, 0)

    l_rest = [load(wm_in.at[:, pl.ds(pl.multiple_of(p * mcols, mcols), mcols)], WM.at[f])]
    far = (full + (1 if rest else 0)) * LANES
    for i, w in enumerate((wg_in, wu_in)):
        for c in range(full):
            col = pl.ds(pl.multiple_of(p * far + c * LANES, LANES), LANES)
            l_rest.append(load(w.at[:, col], WG.at[f, :, pl.ds((2 * c + i) * LANES, LANES)]))
        if rest:
            l_rest.append(load(w.at[:, pl.ds(full * LANES, LANES)], tile.at[i]))
    aligned = full * LANES
    l_rest.append(load(wd_in.at[pl.ds(pl.multiple_of(p * far, LANES), aligned)], WD.at[f, pl.ds(0, aligned)]))
    if rest:
        l_rest.append(load(
            wd_in.at[pl.ds(pl.multiple_of(aligned + p * rest, rest), rest)],
            WD.at[f, pl.ds(aligned, rest)],
        ))


    norm_chunk(p)
    norm_chunk(2 + p)
    for c in l_rest:
        c.wait()
    if rest:
        gate, up = tile[0].astype(F32), tile[1].astype(F32)
        lane = lax.broadcasted_iota(jnp.int32, gate.shape, 1)
        low = jnp.where(lane < rest, gate, pltpu.roll(up, rest, 1))
        high = jnp.where(lane < rest, pltpu.roll(gate, rest, 1), up)
        WG[f, :, 2 * aligned:] = jnp.where(p == 0, low, high).astype(BF16)
    step(0, 2)
    relay(0)
    step(1)
    ts[0].wait_recv()
    norm_chunk(1 - p)
    relay(1)
    step(2, 3, 4)
    ts[1].wait_recv()
    norm_chunk(3 - p)
    arrived(0, 1)

    tap = [taps[pl.ds(i, 1), chan] for i in range(3)]
    pos = lax.rem(lax.broadcasted_iota(jnp.int32, (2 * half, ch), 0), LEN)

    def mix_in(c):
        x = normed[chunk(c), :]

        def proj(q):
            w = WA[:, :, q * ch:(q + 1) * ch].reshape(width, ch)
            return jnp.dot(x, w, preferred_element_type=F32)

        pr = proj(1) * proj(2)
        one = jnp.where(pos >= 1, pltpu.roll(pr, 1, 0), 0.0)
        two = jnp.where(pos >= 2, pltpu.roll(pr, 2, 0), 0.0)
        conv = tap[0] * two + tap[1] * one + tap[2] * pr
        gated[p, chunk(c), :] = (proj(0) * conv).astype(BF16)
        ref = gated.at[p, chunk(c)]
        gz.extend(start(remote(ref, ref, g_s.at[c], g_r.at[c], z_dev)))

    gz, sib, zc, nb = [], [], [], []

    def mix_out(c):
        gz[c].wait_recv()
        g = jnp.concatenate([gated[0, chunk(c), :], gated[1, chunk(c), :]], axis=1)
        for s in range(n_fs):
            MP[chunk(c), s * mcols:(s + 1) * mcols] = jnp.dot(
                g, WM[s], preferred_element_type=F32
            ).astype(BF16)
        sib.extend(start(remote(MP.at[part(c, 1 - t)], RS.at[c], sib_s.at[c], sib_r.at[c], s_dev)))

    def mix_pair(c):
        sib[c].wait_recv()
        BR[p, c] = (MP[part(c, t), :].astype(F32) + RS[c].astype(F32)).astype(BF16)
        zc.extend(start(remote(BR.at[p, c], BR.at[p, c], z_s.at[c], z_r.at[c], z_dev)))

    for c in range(N_CHUNKS):
        mix_in(c)
    arrived(2)
    mix_out(0)
    for c in range(1, N_CHUNKS):
        mix_out(c)
        mix_pair(c - 1)
    mix_pair(N_CHUNKS - 1)

    def stream_chunk(c):
        zc[c].wait_recv()
        step_rows = 32

        def body(i, _):
            rows = pl.ds(pl.multiple_of(i * step_rows, step_rows), step_rows)
            mine = pl.ds(pl.multiple_of((2 * c + t) * half + i * step_rows, step_rows), step_rows)
            branch = jnp.concatenate(
                [BR[q, c, rows, s * mcols:(s + 1) * mcols] for s in range(n_fs) for q in range(2)], axis=1
            )
            stream = tok[mine, :].astype(F32) + branch.astype(F32)
            n2[mine, :] = rms_scale(stream, ffn_gain[...]).astype(BF16)
            return 0

        lax.fori_loop(0, half // step_rows, body, 0)
        ref = n2.at[part(c, t)]
        nb.extend(start(remote(ref, ref, n_s.at[c], n_r.at[c], s_dev)))

    def ffn_piece(k):
        arrived(k)
        _, _, _, c0, nc = pieces[k]

        def body(i, _):
            rows = pl.ds(pl.multiple_of(4 * i * half, 4 * half), 4 * half)
            x = n2[rows, :]
            for a in range(c0, c0 + nc, 2 * LANES):
                n = min(2 * LANES, c0 + nc - a) // 2
                w = WG[:, :, a:a + 2 * n].reshape(width, 2 * n)
                zz = jnp.dot(x, w, preferred_element_type=F32)
                g, u = zz[:, :n], zz[:, n:]
                hidden[rows, a // 2:a // 2 + n] = (g / (1.0 + jnp.exp(-g)) * u).astype(BF16)
            return 0

        lax.fori_loop(0, N_CHUNKS // 2, body, 0)

    step(3, 5)
    stream_chunk(0)
    stream_chunk(1)
    step(4, 6)
    stream_chunk(2)
    stream_chunk(3)
    for c in nb:
        c.wait_recv()
    ffn_piece(3)
    step(5)
    ffn_piece(4)
    step(6, 7, 8)
    ffn_piece(5)
    ffn_piece(6)

    cuts = [pieces[k][3:] for k in (7, 8, 9)]
    blocks = [(f, 0, cols)]
    blocks += [(x_of, *cuts[0]), (y_of, *cuts[0])]
    blocks += [(x_of, *cuts[1]), (y_of, *cuts[1]), (d_of, *cuts[0])]
    blocks += [(x_of, *cuts[2]), (y_of, *cuts[2]), (d_of, *cuts[1]), (d_of, *cuts[2])]
    so, qo = [], []

    def down_send(*ks):
        for k in ks:
            s, c0, nc = blocks[k]
            cs = pl.ds(c0, nc)

            def body(i, _, s=s, c0=c0, nc=nc):
                rows = pl.ds(pl.multiple_of(4 * i * half, 4 * half), 4 * half)
                prod = jnp.dot(
                    hidden[rows, :], WD[s, :, c0:c0 + nc], preferred_element_type=F32
                ).astype(BF16)
                for e in range(4):
                    OP[s, e % 2, 2 * i + e // 2, :, c0:c0 + nc] = prod[e * half:(e + 1) * half]
                return 0

            lax.fori_loop(0, N_CHUNKS // 2, body, 0)
            so.extend(start(remote(
                OP.at[s, 1 - t, :, :, cs], RO.at[s, :, :, cs], o_s.at[k], o_r.at[k], s_dev
            )))

    def down_pair(*ks):
        for k in ks:
            so[k].wait_recv()
            s, c0, nc = blocks[k]
            cs = pl.ds(c0, nc)
            for h in range(2):
                c = 2 * h + 1 - p
                ZC[s, h, :, cs] = (OP[s, t, c, :, cs].astype(F32) + RO[s, c, :, cs].astype(F32)).astype(BF16)
            qo.extend(start(remote(
                ZC.at[s, :, :, cs], RF.at[s, :, :, cs], q_s.at[k], q_r.at[k], z_dev
            )))

    def finish(*ks):
        for k in ks:
            qo[k].wait_recv()
            s, c0, nc = blocks[k]
            for a in range(0, nc, LANES):
                lo = c0 + a
                q, at = lo // mcols, lo % mcols
                cs = pl.ds(lo, LANES)
                ms = pl.ds(pl.multiple_of(s * mcols + at, LANES), LANES)
                whole = pl.ds(pl.multiple_of(s * cols + lo, LANES), LANES)
                for h in range(2):
                    c = 2 * h + p
                    stream = tok[part(c, t), whole].astype(F32) + BR[q, c, :, ms].astype(F32)
                    branch = (
                        OP[s, t, c, :, cs].astype(F32)
                        + RO[s, c, :, cs].astype(F32)
                        + RF[s, h, :, cs].astype(F32)
                    )
                    out[h * half:(h + 1) * half, whole] = (stream + branch).astype(BF16)

    down_send(0)
    step(7, 9)
    down_pair(0)
    down_send(1, 2)
    down_pair(1, 2)
    step(8)
    down_send(3, 4)
    down_pair(3, 4)
    arrived(7)
    down_send(5)
    step(9)
    down_pair(5)
    down_send(6, 7)
    down_pair(6, 7)
    finish(0, 1, 2)
    arrived(8)
    down_send(8)
    down_pair(8)
    finish(3, 4)
    arrived(9)
    down_send(9)
    down_pair(9)
    finish(5, 6, 7, 8, 9)
    for c in sent:
        c.wait_send()


def paired_local(
    tokens, mix_gain, w_gate_b, w_gate_c, w_conv_in, conv_taps, w_mix_out, ffn_gain,
    w_ffn_gate, w_ffn_up, w_ffn_down,
):
    chip_rows, width = tokens.shape
    n_fs = lax.axis_size("fs")
    rows_d = w_gate_b.shape[0]
    ch = w_gate_b.shape[1] // 2
    hid = w_ffn_gate.shape[1] // 2
    cols = w_mix_out.shape[1]
    half = chip_rows // 4
    group = 2 * chip_rows
    n_pieces = len(weight_pieces(rows_d, 3 * ch, cols // 2, 2 * hid, cols, 2 * ch, hid))
    n_blocks = 10
    n_loads = 20 + 2 * (hid // LANES)

    def vmem(*shape):
        return pltpu.VMEM(shape, BF16)

    def dma(*shape):
        return pltpu.SemaphoreType.DMA(shape)

    return pl.pallas_call(
        layer_kernel,
        out_shape=jax.ShapeDtypeStruct((2 * half, width), BF16),
        in_specs=[pl.BlockSpec(memory_space=pl.ANY)] * 11,
        out_specs=pl.BlockSpec(memory_space=pltpu.VMEM),
        scratch_shapes=[
            vmem(group, width),
            vmem(group, width),
            vmem(group, width),
            vmem(n_fs, rows_d, 3 * ch),
            vmem(n_fs, 2 * ch, cols // 2),
            vmem(n_fs, rows_d, 2 * hid),
            vmem(n_fs, hid, cols),
            vmem(2, rows_d, LANES),
            vmem(2, group, ch),
            vmem(group, width // 2),
            vmem(N_CHUNKS, half, width // 2),
            vmem(2, N_CHUNKS, half, width // 2),
            vmem(group, hid),
            vmem(n_fs, 2, N_CHUNKS, half, cols),
            vmem(n_fs, N_CHUNKS, half, cols),
            vmem(n_fs, 2, half, cols),
            vmem(n_fs, 2, half, cols),
            pltpu.VMEM((1, width), F32),
            pltpu.VMEM(conv_taps.shape, F32),
            pltpu.VMEM((1, width), F32),
            dma(n_loads),
            *[dma(n_pieces, 2)] * 4,
            *[dma(2)] * 4,
            *[dma(N_CHUNKS)] * 8,
            *[dma(n_blocks)] * 4,
        ],
        compiler_params=pltpu.CompilerParams(
            collective_id=0, has_side_effects=True, vmem_limit_bytes=60 * 2**20
        ),
    )(
        tokens, w_gate_b, w_gate_c, w_conv_in, w_mix_out, w_ffn_gate, w_ffn_up, w_ffn_down,
        mix_gain.reshape(1, width), conv_taps, ffn_gain.reshape(1, width),
    )


def causal_mix(product_in, conv_taps):
    shaped = product_in.reshape(product_in.shape[0] // LEN, LEN, product_in.shape[1])
    padded = jnp.pad(shaped, ((0, 0), (2, 0), (0, 0)))
    convolved = (
        conv_taps[0] * padded[:, :-2]
        + conv_taps[1] * padded[:, 1:-1]
        + conv_taps[2] * padded[:, 2:]
    )
    return convolved.reshape(product_in.shape)


def general_local(
    tokens, mix_gain, w_gate_b, w_gate_c, w_conv_in, conv_taps, w_mix_out, ffn_gain,
    w_ffn_gate, w_ffn_up, w_ffn_down,
):
    def scatter(product):
        return lax.psum_scatter(
            product.astype(BF16), "tp", scatter_dimension=0, tiled=True
        ).astype(F32)

    def dot(a, b):
        return jnp.dot(a, b, preferred_element_type=F32)

    def rows(w):
        return lax.all_gather(w, "fs", axis=0, tiled=True)

    normed = rms_scale(tokens.astype(F32), mix_gain).astype(BF16)
    gate_b, gate_c, conv_in = (dot(normed, rows(w)) for w in (w_gate_b, w_gate_c, w_conv_in))
    gated = (gate_b * causal_mix(gate_c * conv_in, conv_taps)).astype(BF16)
    row_count = normed.shape[0] // lax.axis_size("tp")
    branch = scatter(dot(gated, lax.all_gather(w_mix_out, "fs", axis=1, tiled=True)))
    own = lax.dynamic_slice_in_dim(tokens, lax.axis_index("tp") * row_count, row_count, 0)
    stream = own.astype(F32) + branch
    normed_two = lax.all_gather(
        rms_scale(stream, ffn_gain).astype(BF16), "tp", axis=0, tiled=True
    )
    hidden = (jax.nn.silu(dot(normed_two, rows(w_ffn_gate))) * dot(normed_two, rows(w_ffn_up))).astype(BF16)
    ffn_branch = scatter(dot(hidden, lax.all_gather(w_ffn_down, "fs", axis=1, tiled=True)))
    return (stream + ffn_branch).astype(BF16)


def solution(mesh):
    in_specs = (
        P(("rep", "fs"), None),
        P(),
        P("fs", "tp"),
        P("fs", "tp"),
        P("fs", "tp"),
        P(None, "tp"),
        P("tp", "fs"),
        P(),
        P("fs", "tp"),
        P("fs", "tp"),
        P("tp", "fs"),
    )
    out_specs = P(("rep", "fs", "tp"), None)
    size = mesh.shape
    square = size["tp"] == 2 and size["fs"] == 4 and size["rep"] % 2 == 0

    def local(*arrays):
        rows, width = arrays[0].shape
        channels, hidden = arrays[2].shape[1], arrays[8].shape[1]
        fits = (
            square
            and rows % (4 * LEN) == 0
            and channels % (2 * LANES) == 0
            and hidden % LANES == 0
            and hidden >= 10 * LANES
            and width % (16 * LANES) == 0
        )
        return (paired_local if fits else general_local)(*arrays)

    return jax.shard_map(local, mesh=mesh, in_specs=in_specs, out_specs=out_specs, check_vma=False)
```

profile of v0, /device:TPU:0, one launch (start us, length us, event | category | flops | bytes accessed | tf_op | source)
XLA Modules:
  0.0 121.8 jit_solution(2258785276280302968)
XLA Ops:
  0.0 119.5 %shard_map.109 = bf16[256,2048]{1,0:T(8,128)(2,1)} custom-call(bf16[512,2048]{1,0:T(8,128)(2,1)} %tokens.1, bf16[512,512]{1,0:T(8,128)(2,1)} %wb.1, bf16[512,512]{1,0:T(8,128)(2,1)} %wc.1, bf16[512,512]{1,0:T(8,128)(2,1)} %wi.1, bf16[512,512]{1,0:T(8,128)(2,1)} %wm_in.1, bf16[512,1408]{1,0:T(8,128)(2,1)} %wg_in.1, bf16[512,1408]{1,0:T(8,128)(2,1)} %wu_in.1, ...), custom_call_target="tpu_custom_call" | custom-call | tf_op jit(solution)/shard_map/pallas_call | solution.py:404
  119.5 2.3 %copy.13 = bf16[256,2048]{1,0:T(8,128)(2,1)} copy(bf16[256,2048]{1,0:T(8,128)(2,1)} %shard_map.109) | data formatting | bytes 2097152
where the time goes:
time: 122 us
  Pallas kernels  120 us (98%)
  local copies, waits for them, and re-layouts  2.3 us (2%)
    pallas_call x1, Pallas kernels, paired_local(): pl.pallas_call(layer_kernel, out_shape=jax.ShapeDtypeStruct((2 * half, wi...  120 us

commit v1 on v0

--- a/solution.py
+++ b/solution.py
@@ -18,40 +18,84 @@
 
 
 N_CHUNKS = 4
-
-
-def weight_pieces(rows_d, n_conv, n_mix, n_gate_up, n_down, mix_rows, down_rows):
-    pieces = [(0, i * rows_d // 2, rows_d // 2, 0, n_conv) for i in range(2)]
-    pieces.append((1, 0, mix_rows, 0, n_mix))
-    units = n_gate_up // (2 * LANES)
-    gate_up = sorted({2 * LANES * u for u in (2 * units // 5, 4 * units // 5, units)} | {0, n_gate_up})
+TILE = 16
+
+
+def inner_units(hidden):
+    units = hidden // LANES
+    return (7 * units + 5) // 11
+
+
+def tiles(rows, share):
+    return int(rows * share) // TILE * TILE
+
+
+def weight_pieces(role, rows_d, n_conv, mix_rows, n_mix, units, hid, n_down):
+    third = 1 / 3
+    pieces = [(0, i * rows_d // 2, rows_d // 2, 0, n_conv, third) for i in range(2)]
+    pieces += [(1, i * mix_rows // 2, mix_rows // 2, 0, n_mix, third) for i in range(2)]
+    cuts = [i * units // 4 for i in range(4)] + [units]
+    if role:
+        cuts = [(2 * i * units + 6) // 7 for i in range(4)] + [units]
+    pieces += [(2, 0, rows_d, 2 * LANES * a, 2 * LANES * (b - a), third) for a, b in zip(cuts, cuts[1:])]
     down = (0, n_down // 2, 3 * n_down // 4, n_down)
-    for weight, rows, cuts in ((2, rows_d, gate_up), (3, down_rows, down)):
-        pieces += [(weight, 0, rows, a, b - a) for a, b in zip(cuts, cuts[1:])]
+    for a, b, share in zip(down, down[1:], (third, 0.29, 0.22)):
+        pieces.append((3, 0, hid, a, b - a, share))
     return pieces
 
 
-def layer_kernel(
+N_PIECES = 11
+
+
+def layer_kernel(*refs):
+    r = lax.axis_index("rep")
+    p = lax.rem(r, 2)
+    f = lax.axis_index("fs")
+    barrier = pltpu.get_barrier_semaphore()
+    x_of = f + 1 - 2 * lax.rem(f, 2)
+    for dev in (
+        {"fs": x_of}, {"fs": lax.rem(f + 2, 4)}, {"rep": r + 1 - 2 * p}, {"tp": 1 - lax.axis_index("tp")}
+    ):
+        pl.semaphore_signal(barrier, inc=1, device_id=dev, device_id_type=MESH)
+    inner = jnp.logical_or(r == 1, r == 2)
+
+    @pl.when(inner)
+    def _():
+        layer_body(1, barrier, *refs)
+
+    @pl.when(jnp.logical_not(inner))
+    def _():
+        layer_body(0, barrier, *refs)
+
+
+def layer_body(
+    role, barrier,
     tokens, wb, wc, wi, wm_in, wg_in, wu_in, wd_in, mix_gain_in, taps_in, ffn_gain_in,
     out,
-    tok, normed, n2, WA, WM, WG, WD, tile, gated, MP, RS, BR, hidden, OP, RO, ZC, RF, mix_gain, taps, ffn_gain,
-    load_sem, ds, dr, fs_, fr, tz_s, tz_r, ts_s, ts_r, g_s, g_r, sib_s, sib_r, z_s, z_r, n_s, n_r,
+    tok, normed, n2, WA, WM, WG, WD, gated, MP, RS, BR, hidden, OP, RO, ZC, RF, mix_gain, taps, ffn_gain,
+    load_sem, ds, dr, fs_, fr, us, ur, tz_s, tz_r, ts_s, ts_r, g_s, g_r, sib_s, sib_r, z_s, z_r, n_s, n_r,
     o_s, o_r, q_s, q_r,
 ):
     n_fs, rows_d, _ = WA.shape
     ch = gated.shape[2]
-    hid = hidden.shape[1]
     width = tokens.shape[1]
     half = tokens.shape[0] // 4
     cols = WD.shape[2]
     mcols = WM.shape[2]
-    full, rest = hid // LANES, hid % LANES
+    all_units = wg_in.shape[1] // LANES
+    units = inner_units(wg_in.shape[1])
+    first = 0
+    if not role:
+        first, units = units, all_units - units
+    hid = units * LANES
 
     r = lax.axis_index("rep")
     f = lax.axis_index("fs")
     t = lax.axis_index("tp")
     p = lax.rem(r, 2)
+    twin = r - 1
     z_dev = {"rep": r + 1 - 2 * p}
+    w_dev = {"rep": 3 - r}
     x_of = f + 1 - 2 * lax.rem(f, 2)
     y_of = lax.rem(f + 2, 4)
     d_of = lax.rem(x_of + 2, 4)
@@ -63,11 +107,10 @@
     def chunk(c):
         return pl.ds(pl.multiple_of(2 * c * half, 2 * half), 2 * half)
 
-    barrier = pltpu.get_barrier_semaphore()
-    for dev in (x_dev, y_dev, z_dev, s_dev):
-        pl.semaphore_signal(barrier, inc=1, device_id=dev, device_id_type=MESH)
-
-    chan = pl.ds(pl.multiple_of(p * ch, ch), ch)
+    if role:
+        pl.semaphore_signal(barrier, inc=1, device_id=w_dev, device_id_type=MESH)
+
+    chan = pl.ds(role * ch, ch)
     loads = []
 
     def load(src, dst):
@@ -89,7 +132,7 @@
     l_small = [
         load(a, b) for a, b in ((mix_gain_in, mix_gain), (taps_in, taps), (ffn_gain_in, ffn_gain))
     ]
-    pl.semaphore_wait(barrier, 4)
+    pl.semaphore_wait(barrier, 4 + role)
 
     def remote(src, dst, s, rcv, dev):
         return pltpu.make_async_remote_copy(
@@ -97,22 +140,45 @@
         )
 
     bufs = (WA, WM, WG, WD)
-    pieces = weight_pieces(rows_d, 3 * ch, mcols, 2 * hid, cols, WM.shape[1], hid)
-
-    def cut(k, slot, first, parts):
-        w, r0, n, c0, nc = pieces[k]
-        return bufs[w].at[slot, pl.ds(r0 + first * n // 2, parts * n // 2), pl.ds(c0, nc)]
+    pieces = weight_pieces(role, rows_d, 3 * ch, WM.shape[1], mcols, units, hid, cols)
+
+    def cut(k, slot, lo, n):
+        w, r0, _, c0, nc, _ = pieces[k]
+        at = r0 + lo
+        if not isinstance(at, int):
+            at = pl.multiple_of(at, TILE)
+        return bufs[w].at[slot, pl.ds(at, n), pl.ds(c0, nc)]
+
+    def share(k):
+        rows = pieces[k][2]
+        lent = tiles(rows, pieces[k][5]) if role else 0
+        kept = rows - lent
+        near = tiles(kept, 0.5)
+        lo = twin * lent if role else 0
+        mine = twin * kept if role else 0
+        return lent, kept, near, lo, mine
 
     def direct(k):
-        ref = cut(k, f, 0, 2)
+        _, kept, _, lo, _ = share(k)
+        ref = cut(k, f, lo, kept)
         return [remote(ref, ref, ds.at[k, c], dr.at[k, c], dev) for c, dev in ((0, x_dev), (1, y_dev))]
 
     def forward(k):
-        a, b = cut(k, x_of, 0, 1), cut(k, y_of, 1, 1)
+        _, kept, near, lo, _ = share(k)
+        a, b = cut(k, x_of, lo, near), cut(k, y_of, lo + near, kept - near)
         return [
             remote(b, b, fs_.at[k, 0], fr.at[k, 0], x_dev),
             remote(a, a, fs_.at[k, 1], fr.at[k, 1], y_dev),
         ]
+
+    def lend(k, *slots):
+        lent, _, _, _, mine = share(k)
+        refs = {0: x_of, 1: y_of, 2: d_of}
+        copies = []
+        for s in slots:
+            ref = cut(k, refs[s], mine, lent)
+            copies.append(remote(ref, ref, us.at[k, s], ur.at[k, s], w_dev))
+        return copies
 
     sent = []
 
@@ -122,7 +188,7 @@
             sent.append(c)
         return copies
 
-    D, F = {}, {}
+    D, F, Z, ZD = {}, {}, {}, {}
 
     def send(*ks):
         for k in ks:
@@ -132,12 +198,33 @@
         for c in D[k]:
             c.wait_recv()
         F[k] = start(*forward(k))
+        if role:
+            Z[k] = start(*lend(k, 0, 1))
         send(*more)
 
+    def across(*ks):
+        for k in ks:
+            if k not in ZD:
+                for c in F[k]:
+                    c.wait_recv()
+                ZD[k] = start(*lend(k, 2)) if role else ()
+
+    def sides(*ks):
+        if role:
+            for k in ks:
+                for c in Z[k]:
+                    c.wait_recv()
+
+    def corner(*ks):
+        across(*ks)
+        for k in ks:
+            for c in ZD[k]:
+                c.wait_recv()
+
     def arrived(*ks):
-        for k in ks:
-            for c in F[k]:
-                c.wait_recv()
+        across(*ks)
+        sides(*ks)
+        corner(*ks)
 
     for k in range(2):
         for c in l_wa[k]:
@@ -163,40 +250,25 @@
 
         lax.fori_loop(0, 2 * half // 64, body, 0)
 
-    l_rest = [load(wm_in.at[:, pl.ds(pl.multiple_of(p * mcols, mcols), mcols)], WM.at[f])]
-    far = (full + (1 if rest else 0)) * LANES
-    for i, w in enumerate((wg_in, wu_in)):
-        for c in range(full):
-            col = pl.ds(pl.multiple_of(p * far + c * LANES, LANES), LANES)
-            l_rest.append(load(w.at[:, col], WG.at[f, :, pl.ds((2 * c + i) * LANES, LANES)]))
-        if rest:
-            l_rest.append(load(w.at[:, pl.ds(full * LANES, LANES)], tile.at[i]))
-    aligned = full * LANES
-    l_rest.append(load(wd_in.at[pl.ds(pl.multiple_of(p * far, LANES), aligned)], WD.at[f, pl.ds(0, aligned)]))
-    if rest:
-        l_rest.append(load(
-            wd_in.at[pl.ds(pl.multiple_of(aligned + p * rest, rest), rest)],
-            WD.at[f, pl.ds(aligned, rest)],
-        ))
-
+    l_rest = [load(wm_in.at[:, pl.ds(role * mcols, mcols)], WM.at[f])]
+    for c in range(units):
+        for i, w in enumerate((wg_in, wu_in)):
+            l_rest.append(load(
+                w.at[:, pl.ds((first + c) * LANES, LANES)], WG.at[f, :, pl.ds((2 * c + i) * LANES, LANES)]
+            ))
+    l_rest.append(load(wd_in.at[pl.ds(first * LANES, hid)], WD.at[f, pl.ds(0, hid)]))
 
     norm_chunk(p)
     norm_chunk(2 + p)
     for c in l_rest:
         c.wait()
-    if rest:
-        gate, up = tile[0].astype(F32), tile[1].astype(F32)
-        lane = lax.broadcasted_iota(jnp.int32, gate.shape, 1)
-        low = jnp.where(lane < rest, gate, pltpu.roll(up, rest, 1))
-        high = jnp.where(lane < rest, pltpu.roll(gate, rest, 1), up)
-        WG[f, :, 2 * aligned:] = jnp.where(p == 0, low, high).astype(BF16)
-    step(0, 2)
+    step(0)
     relay(0)
-    step(1)
+    step(1, 2, 3, *((4,) if role else ()))
     ts[0].wait_recv()
     norm_chunk(1 - p)
+    across(0)
     relay(1)
-    step(2, 3, 4)
     ts[1].wait_recv()
     norm_chunk(3 - p)
     arrived(0, 1)
@@ -215,8 +287,8 @@
         one = jnp.where(pos >= 1, pltpu.roll(pr, 1, 0), 0.0)
         two = jnp.where(pos >= 2, pltpu.roll(pr, 2, 0), 0.0)
         conv = tap[0] * two + tap[1] * one + tap[2] * pr
-        gated[p, chunk(c), :] = (proj(0) * conv).astype(BF16)
-        ref = gated.at[p, chunk(c)]
+        gated[role, chunk(c), :] = (proj(0) * conv).astype(BF16)
+        ref = gated.at[role, chunk(c)]
         gz.extend(start(remote(ref, ref, g_s.at[c], g_r.at[c], z_dev)))
 
     gz, sib, zc, nb = [], [], [], []
@@ -232,17 +304,8 @@
 
     def mix_pair(c):
         sib[c].wait_recv()
-        BR[p, c] = (MP[part(c, t), :].astype(F32) + RS[c].astype(F32)).astype(BF16)
-        zc.extend(start(remote(BR.at[p, c], BR.at[p, c], z_s.at[c], z_r.at[c], z_dev)))
-
-    for c in range(N_CHUNKS):
-        mix_in(c)
-    arrived(2)
-    mix_out(0)
-    for c in range(1, N_CHUNKS):
-        mix_out(c)
-        mix_pair(c - 1)
-    mix_pair(N_CHUNKS - 1)
+        BR[role, c] = (MP[part(c, t), :].astype(F32) + RS[c].astype(F32)).astype(BF16)
+        zc.extend(start(remote(BR.at[role, c], BR.at[role, c], z_s.at[c], z_r.at[c], z_dev)))
 
     def stream_chunk(c):
         zc[c].wait_recv()
@@ -262,39 +325,62 @@
         ref = n2.at[part(c, t)]
         nb.extend(start(remote(ref, ref, n_s.at[c], n_r.at[c], s_dev)))
 
-    def ffn_piece(k):
-        arrived(k)
-        _, _, _, c0, nc = pieces[k]
-
-        def body(i, _):
-            rows = pl.ds(pl.multiple_of(4 * i * half, 4 * half), 4 * half)
-            x = n2[rows, :]
-            for a in range(c0, c0 + nc, 2 * LANES):
-                n = min(2 * LANES, c0 + nc - a) // 2
-                w = WG[:, :, a:a + 2 * n].reshape(width, 2 * n)
-                zz = jnp.dot(x, w, preferred_element_type=F32)
-                g, u = zz[:, :n], zz[:, n:]
-                hidden[rows, a // 2:a // 2 + n] = (g / (1.0 + jnp.exp(-g)) * u).astype(BF16)
-            return 0
-
-        lax.fori_loop(0, N_CHUNKS // 2, body, 0)
-
-    step(3, 5)
+    def ffn_rows(k, i):
+        _, _, _, c0, nc, _ = pieces[k]
+        rows = pl.ds(4 * i * half, 4 * half)
+        x = n2[rows, :]
+        for a in range(c0, c0 + nc, 2 * LANES):
+            w = WG[:, :, a:a + 2 * LANES].reshape(width, 2 * LANES)
+            zz = jnp.dot(x, w, preferred_element_type=F32)
+            g, u = zz[:, :LANES], zz[:, LANES:]
+            hidden[rows, a // 2:a // 2 + LANES] = (g / (1.0 + jnp.exp(-g)) * u).astype(BF16)
+
+    mix_in(0)
+    mix_in(1)
+    step(2)
+    mix_in(2)
+    mix_in(3)
+    step(3, *((5,) if role else (4, 5)))
+    across(1)
+    arrived(2, 3)
+    mix_out(0)
+    mix_out(1)
+    mix_pair(0)
+    mix_out(2)
+    mix_pair(1)
+    step(4, 6)
+    mix_out(3)
+    mix_pair(2)
+    mix_pair(3)
     stream_chunk(0)
+    step(5, 7)
+    across(4)
     stream_chunk(1)
-    step(4, 6)
+    for c in nb[:2]:
+        c.wait_recv()
+    arrived(4)
+    ffn_rows(4, 0)
+    step(6, 8)
+    across(5)
     stream_chunk(2)
+    arrived(5)
+    ffn_rows(5, 0)
     stream_chunk(3)
-    for c in nb:
+    step(7, 9)
+    across(6)
+    for c in nb[2:]:
         c.wait_recv()
-    ffn_piece(3)
-    step(5)
-    ffn_piece(4)
-    step(6, 7, 8)
-    ffn_piece(5)
-    ffn_piece(6)
-
-    cuts = [pieces[k][3:] for k in (7, 8, 9)]
+    ffn_rows(4, 1)
+    ffn_rows(5, 1)
+    arrived(6)
+    ffn_rows(6, 0)
+    ffn_rows(6, 1)
+    step(8, 10)
+    arrived(7)
+    ffn_rows(7, 0)
+    ffn_rows(7, 1)
+
+    cuts = [pieces[k][3:5] for k in (8, 9, 10)]
     blocks = [(f, 0, cols)]
     blocks += [(x_of, *cuts[0]), (y_of, *cuts[0])]
     blocks += [(x_of, *cuts[1]), (y_of, *cuts[1]), (d_of, *cuts[0])]
@@ -309,7 +395,7 @@
             def body(i, _, s=s, c0=c0, nc=nc):
                 rows = pl.ds(pl.multiple_of(4 * i * half, 4 * half), 4 * half)
                 prod = jnp.dot(
-                    hidden[rows, :], WD[s, :, c0:c0 + nc], preferred_element_type=F32
+                    hidden[rows, :hid], WD[s, :hid, c0:c0 + nc], preferred_element_type=F32
                 ).astype(BF16)
                 for e in range(4):
                     OP[s, e % 2, 2 * i + e // 2, :, c0:c0 + nc] = prod[e * half:(e + 1) * half]
@@ -353,25 +439,31 @@
                     out[h * half:(h + 1) * half, whole] = (stream + branch).astype(BF16)
 
     down_send(0)
-    step(7, 9)
+    across(7)
+    step(9)
     down_pair(0)
+    sides(8)
     down_send(1, 2)
     down_pair(1, 2)
-    step(8)
+    across(8)
+    step(10)
+    sides(9)
     down_send(3, 4)
     down_pair(3, 4)
-    arrived(7)
+    across(9)
+    corner(8)
     down_send(5)
-    step(9)
     down_pair(5)
+    across(10)
+    sides(10)
     down_send(6, 7)
     down_pair(6, 7)
     finish(0, 1, 2)
-    arrived(8)
+    corner(9)
     down_send(8)
     down_pair(8)
     finish(3, 4)
-    arrived(9)
+    corner(10)
     down_send(9)
     down_pair(9)
     finish(5, 6, 7, 8, 9)
@@ -387,13 +479,13 @@
     n_fs = lax.axis_size("fs")
     rows_d = w_gate_b.shape[0]
     ch = w_gate_b.shape[1] // 2
-    hid = w_ffn_gate.shape[1] // 2
+    units = inner_units(w_ffn_gate.shape[1])
+    hid = units * LANES
     cols = w_mix_out.shape[1]
     half = chip_rows // 4
     group = 2 * chip_rows
-    n_pieces = len(weight_pieces(rows_d, 3 * ch, cols // 2, 2 * hid, cols, 2 * ch, hid))
     n_blocks = 10
-    n_loads = 20 + 2 * (hid // LANES)
+    n_loads = 15 + 2 * units
 
     def vmem(*shape):
         return pltpu.VMEM(shape, BF16)
@@ -414,7 +506,6 @@
             vmem(n_fs, 2 * ch, cols // 2),
             vmem(n_fs, rows_d, 2 * hid),
             vmem(n_fs, hid, cols),
-            vmem(2, rows_d, LANES),
             vmem(2, group, ch),
             vmem(group, width // 2),
             vmem(N_CHUNKS, half, width // 2),
@@ -428,7 +519,8 @@
             pltpu.VMEM(conv_taps.shape, F32),
             pltpu.VMEM((1, width), F32),
             dma(n_loads),
-            *[dma(n_pieces, 2)] * 4,
+            *[dma(N_PIECES, 2)] * 4,
+            *[dma(N_PIECES, 3)] * 2,
             *[dma(2)] * 4,
             *[dma(N_CHUNKS)] * 8,
             *[dma(n_blocks)] * 4,
@@ -499,7 +591,7 @@
     )
     out_specs = P(("rep", "fs", "tp"), None)
     size = mesh.shape
-    square = size["tp"] == 2 and size["fs"] == 4 and size["rep"] % 2 == 0
+    square = size["tp"] == 2 and size["fs"] == 4 and size["rep"] == 4
 
     def local(*arrays):
         rows, width = arrays[0].shape
@@ -509,7 +601,7 @@
             and rows % (4 * LEN) == 0
             and channels % (2 * LANES) == 0
             and hidden % LANES == 0
-            and hidden >= 10 * LANES
+            and hidden >= 11 * LANES
             and width % (16 * LANES) == 0
         )
         return (paired_local if fits else general_local)(*arrays)

time: 122 us -> 137 us (1.12)
  Pallas kernels: 120 us -> 135 us
    pallas_call x1, Pallas kernels: 120 us -> 135 us  [paired_local(): pl.pallas_call(layer_kernel, out_shape=jax.ShapeDtypeStruct((2 * half, wi...]
where the time goes in v1:
time: 137 us
  Pallas kernels  135 us (99%)
  local copies, waits for them, and re-layouts  2.3 us (2%)
    pallas_call x1, Pallas kernels, paired_local(): pl.pallas_call(layer_kernel, out_shape=jax.ShapeDtypeStruct((2 * half, wi...  135 us

profile of v1, /device:TPU:0, one launch (start us, length us, event | category | flops | bytes accessed | tf_op | source)
XLA Modules:
  0.0 136.9 jit_solution(17603532572220492581)
XLA Ops:
  0.0 134.6 %shard_map.109 = bf16[256,2048]{1,0:T(8,128)(2,1)} custom-call(bf16[512,2048]{1,0:T(8,128)(2,1)} %refs_0_.1, bf16[512,512]{1,0:T(8,128)(2,1)} %refs_1_.1, bf16[512,512]{1,0:T(8,128)(2,1)} %refs_2_.1, bf16[512,512]{1,0:T(8,128)(2,1)} %refs_3_.1, bf16[512,512]{1,0:T(8,128)(2,1)} %refs_4_.1, bf16[512,1408]{1,0:T(8,128)(2,1)} %refs_5_.1, ...), custom_call_target="tpu_custom_call" | custom-call | tf_op jit(solution)/shard_map/pallas_call | solution.py:496
  134.6 2.3 %copy.13 = bf16[256,2048]{1,0:T(8,128)(2,1)} copy(bf16[256,2048]{1,0:T(8,128)(2,1)} %shard_map.109) | data formatting | bytes 2097152

commit v2 on v1

--- a/solution.py
+++ b/solution.py
@@ -36,15 +36,15 @@
     pieces += [(1, i * mix_rows // 2, mix_rows // 2, 0, n_mix, third) for i in range(2)]
     cuts = [i * units // 4 for i in range(4)] + [units]
     if role:
-        cuts = [(2 * i * units + 6) // 7 for i in range(4)] + [units]
-    pieces += [(2, 0, rows_d, 2 * LANES * a, 2 * LANES * (b - a), third) for a, b in zip(cuts, cuts[1:])]
+        cuts = [(u * units + 6) // 7 for u in (0, 1, 3, 5, 6)] + [units]
+    pieces += [(2, 0, rows_d, 2 * LANES * a, 2 * LANES * (b - a), 0.32) for a, b in zip(cuts, cuts[1:])]
     down = (0, n_down // 2, 3 * n_down // 4, n_down)
-    for a, b, share in zip(down, down[1:], (third, 0.29, 0.22)):
+    for a, b, share in zip(down, down[1:], (0.28, 0.25, 0.2)):
         pieces.append((3, 0, hid, a, b - a, share))
     return pieces
 
 
-N_PIECES = 11
+N_PIECES = 12
 
 
 def layer_kernel(*refs):
@@ -71,10 +71,10 @@
 def layer_body(
     role, barrier,
     tokens, wb, wc, wi, wm_in, wg_in, wu_in, wd_in, mix_gain_in, taps_in, ffn_gain_in,
-    out,
-    tok, normed, n2, WA, WM, WG, WD, gated, MP, RS, BR, hidden, OP, RO, ZC, RF, mix_gain, taps, ffn_gain,
+    out_hbm,
+    out, tok, normed, n2, WA, WM, WG, WD, gated, MP, RS, BR, hidden, OP, RO, ZC, RF, mix_gain, taps, ffn_gain,
     load_sem, ds, dr, fs_, fr, us, ur, tz_s, tz_r, ts_s, ts_r, g_s, g_r, sib_s, sib_r, z_s, z_r, n_s, n_r,
-    o_s, o_r, q_s, q_r,
+    o_s, o_r, q_s, q_r, w_s,
 ):
     n_fs, rows_d, _ = WA.shape
     ch = gated.shape[2]
@@ -264,13 +264,26 @@
         c.wait()
     step(0)
     relay(0)
-    step(1, 2, 3, *((4,) if role else ()))
-    ts[0].wait_recv()
-    norm_chunk(1 - p)
-    across(0)
-    relay(1)
-    ts[1].wait_recv()
-    norm_chunk(3 - p)
+    if role:
+        step(1, 2, 3)
+        ts[0].wait_recv()
+        norm_chunk(1 - p)
+        across(0)
+        across(1)
+        step(2)
+        step(3, 4, 5)
+        relay(1)
+        ts[1].wait_recv()
+        norm_chunk(3 - p)
+        across(2)
+        across(3)
+    else:
+        ts[0].wait_recv()
+        norm_chunk(1 - p)
+        step(1, 2, 3)
+        relay(1)
+        ts[1].wait_recv()
+        norm_chunk(3 - p)
     arrived(0, 1)
 
     tap = [taps[pl.ds(i, 1), chan] for i in range(3)]
@@ -327,148 +340,218 @@
 
     def ffn_rows(k, i):
         _, _, _, c0, nc, _ = pieces[k]
-        rows = pl.ds(4 * i * half, 4 * half)
-        x = n2[rows, :]
+        cuts = 2 if nc == 2 * LANES else 1
+        n = 4 * half // cuts
         for a in range(c0, c0 + nc, 2 * LANES):
             w = WG[:, :, a:a + 2 * LANES].reshape(width, 2 * LANES)
-            zz = jnp.dot(x, w, preferred_element_type=F32)
-            g, u = zz[:, :LANES], zz[:, LANES:]
-            hidden[rows, a // 2:a // 2 + LANES] = (g / (1.0 + jnp.exp(-g)) * u).astype(BF16)
-
-    mix_in(0)
-    mix_in(1)
-    step(2)
-    mix_in(2)
-    mix_in(3)
-    step(3, *((5,) if role else (4, 5)))
-    across(1)
-    arrived(2, 3)
-    mix_out(0)
-    mix_out(1)
-    mix_pair(0)
-    mix_out(2)
-    mix_pair(1)
-    step(4, 6)
-    mix_out(3)
-    mix_pair(2)
-    mix_pair(3)
-    stream_chunk(0)
-    step(5, 7)
-    across(4)
-    stream_chunk(1)
-    for c in nb[:2]:
-        c.wait_recv()
-    arrived(4)
-    ffn_rows(4, 0)
-    step(6, 8)
-    across(5)
-    stream_chunk(2)
-    arrived(5)
-    ffn_rows(5, 0)
-    stream_chunk(3)
-    step(7, 9)
-    across(6)
-    for c in nb[2:]:
-        c.wait_recv()
-    ffn_rows(4, 1)
-    ffn_rows(5, 1)
-    arrived(6)
-    ffn_rows(6, 0)
-    ffn_rows(6, 1)
-    step(8, 10)
-    arrived(7)
-    ffn_rows(7, 0)
-    ffn_rows(7, 1)
-
-    cuts = [pieces[k][3:5] for k in (8, 9, 10)]
-    blocks = [(f, 0, cols)]
-    blocks += [(x_of, *cuts[0]), (y_of, *cuts[0])]
-    blocks += [(x_of, *cuts[1]), (y_of, *cuts[1]), (d_of, *cuts[0])]
-    blocks += [(x_of, *cuts[2]), (y_of, *cuts[2]), (d_of, *cuts[1]), (d_of, *cuts[2])]
-    so, qo = [], []
-
-    def down_send(*ks):
-        for k in ks:
-            s, c0, nc = blocks[k]
-            cs = pl.ds(c0, nc)
-
-            def body(i, _, s=s, c0=c0, nc=nc):
-                rows = pl.ds(pl.multiple_of(4 * i * half, 4 * half), 4 * half)
-                prod = jnp.dot(
-                    hidden[rows, :hid], WD[s, :hid, c0:c0 + nc], preferred_element_type=F32
-                ).astype(BF16)
+            for j in range(cuts):
+                rows = pl.ds(4 * i * half + j * n, n)
+                zz = jnp.dot(n2[rows, :], w, preferred_element_type=F32)
+                g, u = zz[:, :LANES], zz[:, LANES:]
+                hidden[rows, a // 2:a // 2 + LANES] = (g / (1.0 + jnp.exp(-g)) * u).astype(BF16)
+
+    dn = range(len(pieces) - 3, len(pieces))
+    cuts = [pieces[k][3:5] for k in dn]
+    groups = [
+        ((f,), (0, cols)), ((x_of, y_of), cuts[0]), ((x_of, y_of), cuts[1]), ((d_of,), cuts[0]),
+        ((x_of, y_of), cuts[2]), ((d_of,), cuts[1]), ((d_of,), cuts[2]),
+    ]
+    so, qo, written = {}, {}, []
+
+    def down_send(k, *hs):
+        slots, (c0, nc) = groups[k]
+        cs = pl.ds(c0, nc)
+        w = jnp.concatenate([WD[s, :hid, c0:c0 + nc] for s in slots], axis=1)
+        for h in hs:
+            prod = jnp.dot(
+                hidden[pl.ds(4 * h * half, 4 * half), :hid], w, preferred_element_type=F32
+            ).astype(BF16)
+            for j, s in enumerate(slots):
                 for e in range(4):
-                    OP[s, e % 2, 2 * i + e // 2, :, c0:c0 + nc] = prod[e * half:(e + 1) * half]
-                return 0
-
-            lax.fori_loop(0, N_CHUNKS // 2, body, 0)
-            so.extend(start(remote(
-                OP.at[s, 1 - t, :, :, cs], RO.at[s, :, :, cs], o_s.at[k], o_r.at[k], s_dev
-            )))
-
-    def down_pair(*ks):
-        for k in ks:
-            so[k].wait_recv()
-            s, c0, nc = blocks[k]
-            cs = pl.ds(c0, nc)
-            for h in range(2):
-                c = 2 * h + 1 - p
+                    OP[s, e % 2, 2 * h + e // 2, :, c0:c0 + nc] = prod[e * half:(e + 1) * half, j * nc:(j + 1) * nc]
+        for h in hs:
+            two = pl.ds(2 * h, 2)
+            so[k, h] = start(*[
+                remote(
+                    OP.at[s, 1 - t, two, :, cs], RO.at[s, two, :, cs], o_s.at[k, h, j], o_r.at[k, h, j], s_dev
+                )
+                for j, s in enumerate(slots)
+            ])
+
+    def down_pair(k, *hs):
+        slots, (c0, nc) = groups[k]
+        cs = pl.ds(c0, nc)
+        for h in hs:
+            c = 2 * h + 1 - p
+            qo[k, h] = []
+            for j, s in enumerate(slots):
+                so[k, h][j].wait_recv()
                 ZC[s, h, :, cs] = (OP[s, t, c, :, cs].astype(F32) + RO[s, c, :, cs].astype(F32)).astype(BF16)
-            qo.extend(start(remote(
-                ZC.at[s, :, :, cs], RF.at[s, :, :, cs], q_s.at[k], q_r.at[k], z_dev
-            )))
-
-    def finish(*ks):
-        for k in ks:
-            qo[k].wait_recv()
-            s, c0, nc = blocks[k]
+                qo[k, h] += start(remote(
+                    ZC.at[s, h, :, cs], RF.at[s, h, :, cs], q_s.at[k, h, j], q_r.at[k, h, j], z_dev
+                ))
+
+    def finish(k, h):
+        slots, (c0, nc) = groups[k]
+        c = 2 * h + p
+        rows = pl.ds(h * half, half)
+        for j, s in enumerate(slots):
+            qo[k, h][j].wait_recv()
             for a in range(0, nc, LANES):
                 lo = c0 + a
                 q, at = lo // mcols, lo % mcols
                 cs = pl.ds(lo, LANES)
                 ms = pl.ds(pl.multiple_of(s * mcols + at, LANES), LANES)
                 whole = pl.ds(pl.multiple_of(s * cols + lo, LANES), LANES)
-                for h in range(2):
-                    c = 2 * h + p
-                    stream = tok[part(c, t), whole].astype(F32) + BR[q, c, :, ms].astype(F32)
-                    branch = (
-                        OP[s, t, c, :, cs].astype(F32)
-                        + RO[s, c, :, cs].astype(F32)
-                        + RF[s, h, :, cs].astype(F32)
-                    )
-                    out[h * half:(h + 1) * half, whole] = (stream + branch).astype(BF16)
-
-    down_send(0)
-    across(7)
-    step(9)
-    down_pair(0)
-    sides(8)
-    down_send(1, 2)
-    down_pair(1, 2)
-    across(8)
-    step(10)
-    sides(9)
-    down_send(3, 4)
-    down_pair(3, 4)
-    across(9)
-    corner(8)
-    down_send(5)
-    down_pair(5)
-    across(10)
-    sides(10)
-    down_send(6, 7)
-    down_pair(6, 7)
-    finish(0, 1, 2)
-    corner(9)
-    down_send(8)
-    down_pair(8)
-    finish(3, 4)
-    corner(10)
-    down_send(9)
-    down_pair(9)
-    finish(5, 6, 7, 8, 9)
+                stream = tok[part(c, t), whole].astype(F32) + BR[q, c, :, ms].astype(F32)
+                branch = (
+                    OP[s, t, c, :, cs].astype(F32)
+                    + RO[s, c, :, cs].astype(F32)
+                    + RF[s, h, :, cs].astype(F32)
+                )
+                out[rows, whole] = (stream + branch).astype(BF16)
+            block = pl.ds(pl.multiple_of(s * cols + c0, LANES), nc)
+            w = pltpu.make_async_copy(out.at[rows, block], out_hbm.at[rows, block], w_s.at[k, h, j])
+            w.start()
+            written.append(w)
+
+    def later(*cs):
+        for c in cs:
+            nb[c].wait_recv()
+
+    if role:
+        mix_in(0)
+        mix_in(1)
+        mix_in(2)
+        step(4, 6)
+        mix_in(3)
+        arrived(2, 3)
+        mix_out(0)
+        mix_out(1)
+        mix_pair(0)
+        step(5, 7)
+        mix_out(2)
+        mix_pair(1)
+        across(4)
+        mix_out(3)
+        mix_pair(2)
+        mix_pair(3)
+        step(6, 8)
+        stream_chunk(0)
+        across(5)
+        stream_chunk(1)
+        step(7)
+        later(0, 1)
+        arrived(4)
+        ffn_rows(4, 0)
+        across(6)
+        arrived(5)
+        ffn_rows(5, 0)
+        stream_chunk(2)
+        step(8, 9, 10)
+        across(7)
+        stream_chunk(3)
+        later(2, 3)
+        arrived(6)
+        ffn_rows(6, 0)
+        across(8)
+        ffn_rows(4, 1)
+        arrived(7)
+        ffn_rows(7, 0)
+        arrived(8)
+        ffn_rows(8, 0)
+        down_send(0, 0)
+        ffn_rows(5, 1)
+        down_pair(0, 0)
+        ffn_rows(6, 1)
+        step(9, 11)
+        ffn_rows(7, 1)
+        ffn_rows(8, 1)
+        down_send(0, 1)
+        step(10)
+        down_pair(0, 1)
+    else:
+        mix_in(0)
+        mix_in(1)
+        step(2)
+        mix_in(2)
+        mix_in(3)
+        step(3, 4, 5)
+        arrived(2, 3)
+        mix_out(0)
+        mix_out(1)
+        mix_pair(0)
+        mix_out(2)
+        mix_pair(1)
+        step(4, 6)
+        mix_out(3)
+        mix_pair(2)
+        mix_pair(3)
+        stream_chunk(0)
+        step(5, 7)
+        stream_chunk(1)
+        later(0, 1)
+        arrived(4)
+        ffn_rows(4, 0)
+        step(6)
+        stream_chunk(2)
+        arrived(5)
+        ffn_rows(5, 0)
+        step(7, 8, 9)
+        stream_chunk(3)
+        later(2, 3)
+        ffn_rows(4, 1)
+        ffn_rows(5, 1)
+        arrived(6)
+        ffn_rows(6, 0)
+        ffn_rows(6, 1)
+        arrived(7)
+        ffn_rows(7, 0)
+        down_send(0, 0)
+        ffn_rows(7, 1)
+        down_pair(0, 0)
+        down_send(0, 1)
+        step(8, 10)
+        down_pair(0, 1)
+        step(9)
+
+    sides(dn[0])
+    down_send(1, 0, 1)
+    down_pair(1, 0, 1)
+    if role:
+        across(dn[0])
+    else:
+        step(dn[2])
+    sides(dn[1])
+    down_send(2, 0, 1)
+    down_pair(2, 0, 1)
+    if role:
+        step(dn[2])
+    corner(dn[0])
+    down_send(3, 0, 1)
+    across(dn[1])
+    down_pair(3, 0, 1)
+    sides(dn[2])
+    down_send(4, 0, 1)
+    finish(0, 0)
+    down_pair(4, 0, 1)
+    across(dn[2])
+    corner(dn[1])
+    down_send(5, 0, 1)
+    finish(0, 1)
+    down_pair(5, 0, 1)
+    corner(dn[2])
+    down_send(6, 0, 1)
+    finish(1, 0)
+    down_pair(6, 0, 1)
+    finish(1, 1)
+    for k in range(2, 7):
+        finish(k, 0)
+        finish(k, 1)
     for c in sent:
         c.wait_send()
+    for c in written:
+        c.wait()
 
 
 def paired_local(
@@ -484,7 +567,6 @@
     cols = w_mix_out.shape[1]
     half = chip_rows // 4
     group = 2 * chip_rows
-    n_blocks = 10
     n_loads = 15 + 2 * units
 
     def vmem(*shape):
@@ -497,8 +579,9 @@
         layer_kernel,
         out_shape=jax.ShapeDtypeStruct((2 * half, width), BF16),
         in_specs=[pl.BlockSpec(memory_space=pl.ANY)] * 11,
-        out_specs=pl.BlockSpec(memory_space=pltpu.VMEM),
+        out_specs=pl.BlockSpec(memory_space=pl.ANY),
         scratch_shapes=[
+            vmem(2 * half, width),
             vmem(group, width),
             vmem(group, width),
             vmem(group, width),
@@ -523,7 +606,7 @@
             *[dma(N_PIECES, 3)] * 2,
             *[dma(2)] * 4,
             *[dma(N_CHUNKS)] * 8,
-            *[dma(n_blocks)] * 4,
+            *[dma(7, 2, 2)] * 5,
         ],
         compiler_params=pltpu.CompilerParams(
             collective_id=0, has_side_effects=True, vmem_limit_bytes=60 * 2**20

time: 137 us -> 116 us (0.85)
  Pallas kernels: 135 us -> 114 us
    pallas_call x1, Pallas kernels: 135 us -> 114 us  [paired_local(): pl.pallas_call(layer_kernel, out_shape=jax.ShapeDtypeStruct((2 * half, wi...]
where the time goes in v2:
time: 116 us
  Pallas kernels  114 us (98%)
  local copies, waits for them, and re-layouts  2.3 us (2%)
    pallas_call x1, Pallas kernels, paired_local(): pl.pallas_call(layer_kernel, out_shape=jax.ShapeDtypeStruct((2 * half, wi...  114 us

profile of v2, /device:TPU:0, one launch (start us, length us, event | category | flops | bytes accessed | tf_op | source)
XLA Modules:
  0.0 115.9 jit_solution(4018269624492316611)
XLA Ops:
  0.0 113.6 %shard_map.109 = bf16[256,2048]{1,0:T(8,128)(2,1)} custom-call(bf16[512,2048]{1,0:T(8,128)(2,1)} %refs_0_.1, bf16[512,512]{1,0:T(8,128)(2,1)} %refs_1_.1, bf16[512,512]{1,0:T(8,128)(2,1)} %refs_2_.1, bf16[512,512]{1,0:T(8,128)(2,1)} %refs_3_.1, bf16[512,512]{1,0:T(8,128)(2,1)} %refs_4_.1, bf16[512,1408]{1,0:T(8,128)(2,1)} %refs_5_.1, ...), custom_call_target="tpu_custom_call" | custom-call | tf_op jit(solution)/shard_map/pallas_call | solution.py:578
  113.6 2.3 %copy.13 = bf16[256,2048]{1,0:T(8,128)(2,1)} copy(bf16[256,2048]{1,0:T(8,128)(2,1)} %shard_map.109) | data formatting | bytes 2097152

commit v3 on v2

--- a/solution.py
+++ b/solution.py
@@ -31,15 +31,14 @@
 
 
 def weight_pieces(role, rows_d, n_conv, mix_rows, n_mix, units, hid, n_down):
-    third = 1 / 3
-    pieces = [(0, i * rows_d // 2, rows_d // 2, 0, n_conv, third) for i in range(2)]
-    pieces += [(1, i * mix_rows // 2, mix_rows // 2, 0, n_mix, third) for i in range(2)]
+    pieces = [(0, i * rows_d // 2, rows_d // 2, 0, n_conv, 0.375) for i in range(2)]
+    pieces += [(1, i * mix_rows // 2, mix_rows // 2, 0, n_mix, 0.375) for i in range(2)]
     cuts = [i * units // 4 for i in range(4)] + [units]
     if role:
         cuts = [(u * units + 6) // 7 for u in (0, 1, 3, 5, 6)] + [units]
     pieces += [(2, 0, rows_d, 2 * LANES * a, 2 * LANES * (b - a), 0.32) for a, b in zip(cuts, cuts[1:])]
     down = (0, n_down // 2, 3 * n_down // 4, n_down)
-    for a, b, share in zip(down, down[1:], (0.28, 0.25, 0.2)):
+    for a, b, share in zip(down, down[1:], (0, 0.25, 0.2)):
         pieces.append((3, 0, hid, a, b - a, share))
     return pieces
 
@@ -73,8 +72,7 @@
     tokens, wb, wc, wi, wm_in, wg_in, wu_in, wd_in, mix_gain_in, taps_in, ffn_gain_in,
     out_hbm,
     out, tok, normed, n2, WA, WM, WG, WD, gated, MP, RS, BR, hidden, OP, RO, ZC, RF, mix_gain, taps, ffn_gain,
-    load_sem, ds, dr, fs_, fr, us, ur, tz_s, tz_r, ts_s, ts_r, g_s, g_r, sib_s, sib_r, z_s, z_r, n_s, n_r,
-    o_s, o_r, q_s, q_r, w_s,
+    load_sem, gone, dr, fr, ur, cr, tz_r, ts_r, g_r, sib_r, z_r, n_r, o_r, q_r,
 ):
     n_fs, rows_d, _ = WA.shape
     ch = gated.shape[2]
@@ -111,27 +109,22 @@
         pl.semaphore_signal(barrier, inc=1, device_id=w_dev, device_id_type=MESH)
 
     chan = pl.ds(role * ch, ch)
-    loads = []
-
-    def load(src, dst):
-        c = pltpu.make_async_copy(src, dst, load_sem.at[len(loads)])
-        c.start()
-        loads.append(c)
-        return c
-
-    l_wa = []
+    def load(src, dst, k):
+        pltpu.make_async_copy(src, dst, load_sem.at[k]).start()
+
+    def loaded(ref, k):
+        pltpu.make_async_copy(ref, ref, load_sem.at[k]).wait()
+
+    w_rows = [pl.ds(k * (rows_d // 2), rows_d // 2) for k in range(2)]
     for k in range(2):
-        rows = pl.ds(k * (rows_d // 2), rows_d // 2)
-        l_wa.append([
-            load(w.at[rows, chan], WA.at[f, rows, pl.ds(i * ch, ch)]) for i, w in enumerate((wb, wc, wi))
-        ])
-    l_tok = [
-        load(tokens.at[pl.ds((2 * core + h) * half, half)], tok.at[part(2 * h + p, core)])
-        for h in range(2) for core in range(2)
-    ]
-    l_small = [
-        load(a, b) for a, b in ((mix_gain_in, mix_gain), (taps_in, taps), (ffn_gain_in, ffn_gain))
-    ]
+        for i, w in enumerate((wb, wc, wi)):
+            load(w.at[w_rows[k], chan], WA.at[f, w_rows[k], pl.ds(i * ch, ch)], k)
+    for h in range(2):
+        for core in range(2):
+            load(tokens.at[pl.ds((2 * core + h) * half, half)], tok.at[part(2 * h + p, core)], 2)
+    small = ((mix_gain_in, mix_gain), (taps_in, taps), (ffn_gain_in, ffn_gain))
+    for i, (src, dst) in enumerate(small):
+        load(src, dst, 3 + i)
     pl.semaphore_wait(barrier, 4 + role)
 
     def remote(src, dst, s, rcv, dev):
@@ -161,65 +154,65 @@
     def direct(k):
         _, kept, _, lo, _ = share(k)
         ref = cut(k, f, lo, kept)
-        return [remote(ref, ref, ds.at[k, c], dr.at[k, c], dev) for c, dev in ((0, x_dev), (1, y_dev))]
+        sem = gone.at[pieces[k][0]]
+        return [remote(ref, ref, sem, dr.at[k], dev) for dev in (x_dev, y_dev)]
 
     def forward(k):
         _, kept, near, lo, _ = share(k)
         a, b = cut(k, x_of, lo, near), cut(k, y_of, lo + near, kept - near)
         return [
-            remote(b, b, fs_.at[k, 0], fr.at[k, 0], x_dev),
-            remote(a, a, fs_.at[k, 1], fr.at[k, 1], y_dev),
+            remote(b, b, gone.at[pieces[k][0]], fr.at[k], x_dev),
+            remote(a, a, gone.at[pieces[k][0]], fr.at[k], y_dev),
         ]
 
-    def lend(k, *slots):
+    def lend(k, sems, *slots):
         lent, _, _, _, mine = share(k)
-        refs = {0: x_of, 1: y_of, 2: d_of}
-        copies = []
-        for s in slots:
-            ref = cut(k, refs[s], mine, lent)
-            copies.append(remote(ref, ref, us.at[k, s], ur.at[k, s], w_dev))
-        return copies
-
-    sent = []
+        if not lent:
+            return []
+        refs = [cut(k, slot, mine, lent) for slot in slots]
+        return [remote(ref, ref, gone.at[pieces[k][0]], sems.at[k], w_dev) for ref in refs]
 
     def start(*copies):
         for c in copies:
             c.start()
-            sent.append(c)
-        return copies
-
-    D, F, Z, ZD = {}, {}, {}, {}
+
+    def landed(ref, sem):
+        remote(ref, ref, sem, sem, s_dev).wait_recv()
+
+    def left(ref, k):
+        remote(ref, ref, gone.at[k], gone.at[k], s_dev).wait_send()
+
+    passed = set()
 
     def send(*ks):
         for k in ks:
-            D[k] = start(*direct(k))
+            start(*direct(k))
 
     def step(k, *more):
-        for c in D[k]:
-            c.wait_recv()
-        F[k] = start(*forward(k))
+        landed(cut(k, pl.ds(0, 2), 0, share(k)[1]), dr.at[k])
+        start(*forward(k))
         if role:
-            Z[k] = start(*lend(k, 0, 1))
+            start(*lend(k, ur, x_of, y_of))
         send(*more)
 
     def across(*ks):
         for k in ks:
-            if k not in ZD:
-                for c in F[k]:
-                    c.wait_recv()
-                ZD[k] = start(*lend(k, 2)) if role else ()
+            if k not in passed:
+                passed.add(k)
+                landed(cut(k, 0, 0, share(k)[1]), fr.at[k])
+                if role:
+                    start(*lend(k, cr, d_of))
 
     def sides(*ks):
-        if role:
-            for k in ks:
-                for c in Z[k]:
-                    c.wait_recv()
+        for k in ks:
+            if share(k)[0]:
+                landed(cut(k, pl.ds(0, 2), 0, share(k)[0]), ur.at[k])
 
     def corner(*ks):
         across(*ks)
         for k in ks:
-            for c in ZD[k]:
-                c.wait_recv()
+            if share(k)[0]:
+                landed(cut(k, 0, 0, share(k)[0]), cr.at[k])
 
     def arrived(*ks):
         across(*ks)
@@ -227,20 +220,22 @@
         corner(*ks)
 
     for k in range(2):
-        for c in l_wa[k]:
-            c.wait()
+        loaded(WA.at[f, w_rows[k]], k)
         send(k)
-    for c in l_tok + l_small:
-        c.wait()
-    tz, ts = [], []
+    loaded(tok.at[pl.ds(0, 4 * half)], 2)
+    for i, (_, dst) in enumerate(small):
+        loaded(dst, 3 + i)
     for h in range(2):
         ref = tok.at[part(2 * h + p, t)]
-        tz += start(remote(ref, ref, tz_s.at[h], tz_r.at[h], z_dev))
+        start(remote(ref, ref, gone.at[4], tz_r.at[h], z_dev))
 
     def relay(h):
-        tz[h].wait_recv()
         ref = tok.at[part(2 * h + 1 - p, t)]
-        ts.extend(start(remote(ref, ref, ts_s.at[h], ts_r.at[h], s_dev)))
+        landed(ref, tz_r.at[h])
+        start(remote(ref, ref, gone.at[5], ts_r.at[h], s_dev))
+
+    def sibling(h):
+        landed(tok.at[part(2 * h, t)], ts_r.at[h])
 
     def norm_chunk(c):
         def body(i, _):
@@ -250,39 +245,38 @@
 
         lax.fori_loop(0, 2 * half // 64, body, 0)
 
-    l_rest = [load(wm_in.at[:, pl.ds(role * mcols, mcols)], WM.at[f])]
+    load(wm_in.at[:, pl.ds(role * mcols, mcols)], WM.at[f], 6)
     for c in range(units):
         for i, w in enumerate((wg_in, wu_in)):
-            l_rest.append(load(
-                w.at[:, pl.ds((first + c) * LANES, LANES)], WG.at[f, :, pl.ds((2 * c + i) * LANES, LANES)]
-            ))
-    l_rest.append(load(wd_in.at[pl.ds(first * LANES, hid)], WD.at[f, pl.ds(0, hid)]))
+            load(w.at[:, pl.ds((first + c) * LANES, LANES)], WG.at[f, :, pl.ds((2 * c + i) * LANES, LANES)], 7)
+    load(wd_in.at[pl.ds(first * LANES, hid)], WD.at[f, pl.ds(0, hid)], 8)
 
     norm_chunk(p)
     norm_chunk(2 + p)
-    for c in l_rest:
-        c.wait()
+    loaded(WM.at[f], 6)
+    loaded(WG.at[f, :, pl.ds(0, 2 * hid)], 7)
+    loaded(WD.at[f, pl.ds(0, hid)], 8)
     step(0)
     relay(0)
     if role:
         step(1, 2, 3)
-        ts[0].wait_recv()
+        sibling(0)
         norm_chunk(1 - p)
         across(0)
         across(1)
         step(2)
         step(3, 4, 5)
         relay(1)
-        ts[1].wait_recv()
+        sibling(1)
         norm_chunk(3 - p)
         across(2)
         across(3)
     else:
-        ts[0].wait_recv()
+        sibling(0)
         norm_chunk(1 - p)
         step(1, 2, 3)
         relay(1)
-        ts[1].wait_recv()
+        sibling(1)
         norm_chunk(3 - p)
     arrived(0, 1)
 
@@ -302,26 +296,24 @@
         conv = tap[0] * two + tap[1] * one + tap[2] * pr
         gated[role, chunk(c), :] = (proj(0) * conv).astype(BF16)
         ref = gated.at[role, chunk(c)]
-        gz.extend(start(remote(ref, ref, g_s.at[c], g_r.at[c], z_dev)))
-
-    gz, sib, zc, nb = [], [], [], []
+        start(remote(ref, ref, gone.at[6], g_r.at[c], z_dev))
 
     def mix_out(c):
-        gz[c].wait_recv()
+        landed(gated.at[role, chunk(c)], g_r.at[c])
         g = jnp.concatenate([gated[0, chunk(c), :], gated[1, chunk(c), :]], axis=1)
         for s in range(n_fs):
             MP[chunk(c), s * mcols:(s + 1) * mcols] = jnp.dot(
                 g, WM[s], preferred_element_type=F32
             ).astype(BF16)
-        sib.extend(start(remote(MP.at[part(c, 1 - t)], RS.at[c], sib_s.at[c], sib_r.at[c], s_dev)))
+        start(remote(MP.at[part(c, 1 - t)], RS.at[c], gone.at[7], sib_r.at[c], s_dev))
 
     def mix_pair(c):
-        sib[c].wait_recv()
+        landed(RS.at[c], sib_r.at[c])
         BR[role, c] = (MP[part(c, t), :].astype(F32) + RS[c].astype(F32)).astype(BF16)
-        zc.extend(start(remote(BR.at[role, c], BR.at[role, c], z_s.at[c], z_r.at[c], z_dev)))
+        start(remote(BR.at[role, c], BR.at[role, c], gone.at[8], z_r.at[c], z_dev))
 
     def stream_chunk(c):
-        zc[c].wait_recv()
+        landed(BR.at[1 - role, c], z_r.at[c])
         step_rows = 32
 
         def body(i, _):
@@ -336,7 +328,7 @@
 
         lax.fori_loop(0, half // step_rows, body, 0)
         ref = n2.at[part(c, t)]
-        nb.extend(start(remote(ref, ref, n_s.at[c], n_r.at[c], s_dev)))
+        start(remote(ref, ref, gone.at[9], n_r.at[c], s_dev))
 
     def ffn_rows(k, i):
         _, _, _, c0, nc, _ = pieces[k]
@@ -356,11 +348,13 @@
         ((f,), (0, cols)), ((x_of, y_of), cuts[0]), ((x_of, y_of), cuts[1]), ((d_of,), cuts[0]),
         ((x_of, y_of), cuts[2]), ((d_of,), cuts[1]), ((d_of,), cuts[2]),
     ]
-    so, qo, written = {}, {}, []
+    def span(k, hs):
+        n = len(groups[k][0])
+        return n, pl.ds(*groups[k][1]), pl.ds(2 * hs[0], 2 * len(hs)), pl.ds(hs[0], len(hs)), 7 * hs[0] + k
 
     def down_send(k, *hs):
         slots, (c0, nc) = groups[k]
-        cs = pl.ds(c0, nc)
+        _, cs, two, _, sem = span(k, hs)
         w = jnp.concatenate([WD[s, :hid, c0:c0 + nc] for s in slots], axis=1)
         for h in hs:
             prod = jnp.dot(
@@ -369,55 +363,46 @@
             for j, s in enumerate(slots):
                 for e in range(4):
                     OP[s, e % 2, 2 * h + e // 2, :, c0:c0 + nc] = prod[e * half:(e + 1) * half, j * nc:(j + 1) * nc]
-        for h in hs:
-            two = pl.ds(2 * h, 2)
-            so[k, h] = start(*[
-                remote(
-                    OP.at[s, 1 - t, two, :, cs], RO.at[s, two, :, cs], o_s.at[k, h, j], o_r.at[k, h, j], s_dev
-                )
-                for j, s in enumerate(slots)
-            ])
+        for s in slots:
+            start(remote(OP.at[s, 1 - t, two, :, cs], RO.at[s, two, :, cs], gone.at[10], o_r.at[sem], s_dev))
 
     def down_pair(k, *hs):
+        slots, _ = groups[k]
+        n, cs, two, rows, sem = span(k, hs)
+        landed(RO.at[pl.ds(0, n), two, :, cs], o_r.at[sem])
+        for s in slots:
+            for h in hs:
+                c = 2 * h + 1 - p
+                ZC[s, h, :, cs] = (OP[s, t, c, :, cs].astype(F32) + RO[s, c, :, cs].astype(F32)).astype(BF16)
+            start(remote(ZC.at[s, rows, :, cs], RF.at[s, rows, :, cs], gone.at[11], q_r.at[sem], z_dev))
+
+    def finish(k, *hs):
         slots, (c0, nc) = groups[k]
-        cs = pl.ds(c0, nc)
-        for h in hs:
-            c = 2 * h + 1 - p
-            qo[k, h] = []
-            for j, s in enumerate(slots):
-                so[k, h][j].wait_recv()
-                ZC[s, h, :, cs] = (OP[s, t, c, :, cs].astype(F32) + RO[s, c, :, cs].astype(F32)).astype(BF16)
-                qo[k, h] += start(remote(
-                    ZC.at[s, h, :, cs], RF.at[s, h, :, cs], q_s.at[k, h, j], q_r.at[k, h, j], z_dev
-                ))
-
-    def finish(k, h):
-        slots, (c0, nc) = groups[k]
-        c = 2 * h + p
-        rows = pl.ds(h * half, half)
-        for j, s in enumerate(slots):
-            qo[k, h][j].wait_recv()
-            for a in range(0, nc, LANES):
-                lo = c0 + a
-                q, at = lo // mcols, lo % mcols
-                cs = pl.ds(lo, LANES)
-                ms = pl.ds(pl.multiple_of(s * mcols + at, LANES), LANES)
-                whole = pl.ds(pl.multiple_of(s * cols + lo, LANES), LANES)
-                stream = tok[part(c, t), whole].astype(F32) + BR[q, c, :, ms].astype(F32)
-                branch = (
-                    OP[s, t, c, :, cs].astype(F32)
-                    + RO[s, c, :, cs].astype(F32)
-                    + RF[s, h, :, cs].astype(F32)
-                )
-                out[rows, whole] = (stream + branch).astype(BF16)
+        n, cs, _, rows, sem = span(k, hs)
+        landed(RF.at[pl.ds(0, n), rows, :, cs], q_r.at[sem])
+        for s in slots:
+            for h in hs:
+                c = 2 * h + p
+                for a in range(0, nc, LANES):
+                    lo = c0 + a
+                    q, at = lo // mcols, lo % mcols
+                    cs = pl.ds(lo, LANES)
+                    ms = pl.ds(pl.multiple_of(s * mcols + at, LANES), LANES)
+                    whole = pl.ds(pl.multiple_of(s * cols + lo, LANES), LANES)
+                    stream = tok[part(c, t), whole].astype(F32) + BR[q, c, :, ms].astype(F32)
+                    branch = (
+                        OP[s, t, c, :, cs].astype(F32)
+                        + RO[s, c, :, cs].astype(F32)
+                        + RF[s, h, :, cs].astype(F32)
+                    )
+                    out[h * half:(h + 1) * half, whole] = (stream + branch).astype(BF16)
+            lines = pl.ds(hs[0] * half, len(hs) * half)
             block = pl.ds(pl.multiple_of(s * cols + c0, LANES), nc)
-            w = pltpu.make_async_copy(out.at[rows, block], out_hbm.at[rows, block], w_s.at[k, h, j])
-            w.start()
-            written.append(w)
+            pltpu.make_async_copy(out.at[lines, block], out_hbm.at[lines, block], load_sem.at[9]).start()
 
     def later(*cs):
         for c in cs:
-            nb[c].wait_recv()
+            landed(n2.at[part(c, 1 - t)], n_r.at[c])
 
     if role:
         mix_in(0)
@@ -448,7 +433,7 @@
         arrived(5)
         ffn_rows(5, 0)
         stream_chunk(2)
-        step(8, 9, 10)
+        step(8, 9, 10, 11)
         across(7)
         stream_chunk(3)
         later(2, 3)
@@ -464,7 +449,7 @@
         ffn_rows(5, 1)
         down_pair(0, 0)
         ffn_rows(6, 1)
-        step(9, 11)
+        step(9)
         ffn_rows(7, 1)
         ffn_rows(8, 1)
         down_send(0, 1)
@@ -519,39 +504,39 @@
     down_send(1, 0, 1)
     down_pair(1, 0, 1)
     if role:
-        across(dn[0])
-    else:
         step(dn[2])
     sides(dn[1])
     down_send(2, 0, 1)
     down_pair(2, 0, 1)
-    if role:
+    across(dn[0])
+    if not role:
         step(dn[2])
+    finish(0, 0)
+    sides(dn[2])
+    down_send(4, 0, 1)
+    down_pair(4, 0, 1)
     corner(dn[0])
     down_send(3, 0, 1)
+    finish(0, 1)
     across(dn[1])
     down_pair(3, 0, 1)
-    sides(dn[2])
-    down_send(4, 0, 1)
-    finish(0, 0)
-    down_pair(4, 0, 1)
-    across(dn[2])
     corner(dn[1])
     down_send(5, 0, 1)
-    finish(0, 1)
+    across(dn[2])
     down_pair(5, 0, 1)
     corner(dn[2])
     down_send(6, 0, 1)
-    finish(1, 0)
+    finish(1, 0, 1)
     down_pair(6, 0, 1)
-    finish(1, 1)
-    for k in range(2, 7):
-        finish(k, 0)
-        finish(k, 1)
-    for c in sent:
-        c.wait_send()
-    for c in written:
-        c.wait()
+    for k in (2, 4, 3, 5, 6):
+        finish(k, 0, 1)
+    for w, ref in enumerate((
+        WA.at[pl.ds(0, 3)], WM.at[pl.ds(0, 3)], WG.at[pl.ds(0, 3), :, pl.ds(0, 2 * hid)],
+        WD.at[pl.ds(0, 3), pl.ds(0, hid)], tok.at[pl.ds(0, 2 * half)], tok.at[pl.ds(0, 2 * half)],
+        gated.at[role], RS, BR.at[role], n2.at[pl.ds(0, 4 * half)], RO, ZC,
+    )):
+        left(ref, w)
+    loaded(out, 9)
 
 
 def paired_local(
@@ -567,7 +552,6 @@
     cols = w_mix_out.shape[1]
     half = chip_rows // 4
     group = 2 * chip_rows
-    n_loads = 15 + 2 * units
 
     def vmem(*shape):
         return pltpu.VMEM(shape, BF16)
@@ -601,12 +585,12 @@
             pltpu.VMEM((1, width), F32),
             pltpu.VMEM(conv_taps.shape, F32),
             pltpu.VMEM((1, width), F32),
-            dma(n_loads),
-            *[dma(N_PIECES, 2)] * 4,
-            *[dma(N_PIECES, 3)] * 2,
-            *[dma(2)] * 4,
-            *[dma(N_CHUNKS)] * 8,
-            *[dma(7, 2, 2)] * 5,
+            dma(10),
+            dma(12),
+            *[dma(N_PIECES)] * 4,
+            *[dma(2)] * 2,
+            *[dma(N_CHUNKS)] * 4,
+            *[dma(14)] * 2,
         ],
         compiler_params=pltpu.CompilerParams(
             collective_id=0, has_side_effects=True, vmem_limit_bytes=60 * 2**20

time: 116 us -> 110 us (0.948)
  Pallas kernels: 114 us -> 108 us
    pallas_call x1, Pallas kernels: 114 us -> 108 us  [paired_local(): pl.pallas_call(layer_kernel, out_shape=jax.ShapeDtypeStruct((2 * half, wi...]
where the time goes in v3:
time: 110 us
  Pallas kernels  108 us (98%)
  local copies, waits for them, and re-layouts  2.3 us (2%)
    pallas_call x1, Pallas kernels, paired_local(): pl.pallas_call(layer_kernel, out_shape=jax.ShapeDtypeStruct((2 * half, wi...  108 us
    unnamed x1, local copies, waits for them, and re-layouts  2.3 us

profile of v3, /device:TPU:0, one launch (start us, length us, event | category | flops | bytes accessed | tf_op | source)
XLA Modules:
  0.0 110.1 jit_solution(8955691948035213061)
XLA Ops:
  0.0 107.8 %shard_map.109 = bf16[256,2048]{1,0:T(8,128)(2,1)} custom-call(bf16[512,2048]{1,0:T(8,128)(2,1)} %refs_0_.1, bf16[512,512]{1,0:T(8,128)(2,1)} %refs_1_.1, bf16[512,512]{1,0:T(8,128)(2,1)} %refs_2_.1, bf16[512,512]{1,0:T(8,128)(2,1)} %refs_3_.1, bf16[512,512]{1,0:T(8,128)(2,1)} %refs_4_.1, bf16[512,1408]{1,0:T(8,128)(2,1)} %refs_5_.1, ...), custom_call_target="tpu_custom_call" | custom-call | tf_op jit(solution)/shard_map/pallas_call | solution.py:562
  107.8 2.3 %copy.13 = bf16[256,2048]{1,0:T(8,128)(2,1)} copy(bf16[256,2048]{1,0:T(8,128)(2,1)} %shard_map.109) | data formatting | bytes 2097152

commit v4 on v3

--- a/solution.py
+++ b/solution.py
@@ -30,8 +30,16 @@
     return int(rows * share) // TILE * TILE
 
 
+def head_rows(role, rows):
+    if role:
+        return [0, rows // 4, 5 * rows // 8, rows]
+    return [0, rows // 2, rows]
+
+
 def weight_pieces(role, rows_d, n_conv, mix_rows, n_mix, units, hid, n_down):
-    pieces = [(0, i * rows_d // 2, rows_d // 2, 0, n_conv, 0.375) for i in range(2)]
+    starts = head_rows(role, rows_d)
+    head = [(0, a, b - a, 0, n_conv, 0.375) for a, b in zip(starts, starts[1:])]
+    pieces = head[:2]
     pieces += [(1, i * mix_rows // 2, mix_rows // 2, 0, n_mix, 0.375) for i in range(2)]
     cuts = [i * units // 4 for i in range(4)] + [units]
     if role:
@@ -40,10 +48,10 @@
     down = (0, n_down // 2, 3 * n_down // 4, n_down)
     for a, b, share in zip(down, down[1:], (0, 0.25, 0.2)):
         pieces.append((3, 0, hid, a, b - a, share))
-    return pieces
-
-
-N_PIECES = 12
+    return pieces + head[2:]
+
+
+N_PIECES = 13
 
 
 def layer_kernel(*refs):
@@ -70,8 +78,8 @@
 def layer_body(
     role, barrier,
     tokens, wb, wc, wi, wm_in, wg_in, wu_in, wd_in, mix_gain_in, taps_in, ffn_gain_in,
-    out_hbm,
-    out, tok, normed, n2, WA, WM, WG, WD, gated, MP, RS, BR, hidden, OP, RO, ZC, RF, mix_gain, taps, ffn_gain,
+    out,
+    tok, normed, n2, WA, WM, WG, WD, gated, MP, RS, BR, hidden, OP, RO, ZC, RF, mix_gain, taps, ffn_gain,
     load_sem, gone, dr, fr, ur, cr, tz_r, ts_r, g_r, sib_r, z_r, n_r, o_r, q_r,
 ):
     n_fs, rows_d, _ = WA.shape
@@ -115,10 +123,11 @@
     def loaded(ref, k):
         pltpu.make_async_copy(ref, ref, load_sem.at[k]).wait()
 
-    w_rows = [pl.ds(k * (rows_d // 2), rows_d // 2) for k in range(2)]
-    for k in range(2):
+    starts = head_rows(role, rows_d)
+    w_rows = [pl.ds(a, b - a) for a, b in zip(starts, starts[1:])]
+    for k in range(len(w_rows)):
         for i, w in enumerate((wb, wc, wi)):
-            load(w.at[w_rows[k], chan], WA.at[f, w_rows[k], pl.ds(i * ch, ch)], k)
+            load(w.at[w_rows[k], chan], WA.at[f, w_rows[k], pl.ds(i * ch, ch)], (0, 1, 10)[k])
     for h in range(2):
         for core in range(2):
             load(tokens.at[pl.ds((2 * core + h) * half, half)], tok.at[part(2 * h + p, core)], 2)
@@ -219,9 +228,9 @@
         sides(*ks)
         corner(*ks)
 
-    for k in range(2):
-        loaded(WA.at[f, w_rows[k]], k)
-        send(k)
+    for k in range(len(w_rows)):
+        loaded(WA.at[f, w_rows[k]], (0, 1, 10)[k])
+        send((0, 1, 12)[k])
     loaded(tok.at[pl.ds(0, 4 * half)], 2)
     for i, (_, dst) in enumerate(small):
         loaded(dst, 3 + i)
@@ -257,13 +266,16 @@
     loaded(WG.at[f, :, pl.ds(0, 2 * hid)], 7)
     loaded(WD.at[f, pl.ds(0, hid)], 8)
     step(0)
+    if role:
+        step(1)
     relay(0)
     if role:
-        step(1, 2, 3)
+        step(12, 2, 3)
         sibling(0)
         norm_chunk(1 - p)
         across(0)
         across(1)
+        across(12)
         step(2)
         step(3, 4, 5)
         relay(1)
@@ -278,7 +290,7 @@
         relay(1)
         sibling(1)
         norm_chunk(3 - p)
-    arrived(0, 1)
+    arrived(0, 1, *((12,) if role else ()))
 
     tap = [taps[pl.ds(i, 1), chan] for i in range(3)]
     pos = lax.rem(lax.broadcasted_iota(jnp.int32, (2 * half, ch), 0), LEN)
@@ -342,7 +354,7 @@
                 g, u = zz[:, :LANES], zz[:, LANES:]
                 hidden[rows, a // 2:a // 2 + LANES] = (g / (1.0 + jnp.exp(-g)) * u).astype(BF16)
 
-    dn = range(len(pieces) - 3, len(pieces))
+    dn = (9, 10, 11) if role else (8, 9, 10)
     cuts = [pieces[k][3:5] for k in dn]
     groups = [
         ((f,), (0, cols)), ((x_of, y_of), cuts[0]), ((x_of, y_of), cuts[1]), ((d_of,), cuts[0]),
@@ -396,9 +408,6 @@
                         + RF[s, h, :, cs].astype(F32)
                     )
                     out[h * half:(h + 1) * half, whole] = (stream + branch).astype(BF16)
-            lines = pl.ds(hs[0] * half, len(hs) * half)
-            block = pl.ds(pl.multiple_of(s * cols + c0, LANES), nc)
-            pltpu.make_async_copy(out.at[lines, block], out_hbm.at[lines, block], load_sem.at[9]).start()
 
     def later(*cs):
         for c in cs:
@@ -437,24 +446,45 @@
         across(7)
         stream_chunk(3)
         later(2, 3)
+        ffn_rows(4, 1)
+        ffn_rows(5, 1)
+        across(8)
         arrived(6)
         ffn_rows(6, 0)
-        across(8)
-        ffn_rows(4, 1)
+        ffn_rows(6, 1)
         arrived(7)
         ffn_rows(7, 0)
         arrived(8)
         ffn_rows(8, 0)
         down_send(0, 0)
-        ffn_rows(5, 1)
-        down_pair(0, 0)
-        ffn_rows(6, 1)
-        step(9)
         ffn_rows(7, 1)
         ffn_rows(8, 1)
+        down_pair(0, 0)
         down_send(0, 1)
+        step(9)
+        sides(9)
+        down_send(1, 0, 1)
+        down_pair(0, 1)
+        down_pair(1, 0, 1)
         step(10)
-        down_pair(0, 1)
+        finish(0, 0)
+        step(11)
+        sides(10)
+        down_send(2, 0, 1)
+        finish(0, 1)
+        down_pair(2, 0, 1)
+        sides(11)
+        down_send(4, 0, 1)
+        across(9)
+        down_send(3, 0, 1)
+        down_pair(4, 0, 1)
+        across(10)
+        down_pair(3, 0, 1)
+        corner(10)
+        down_send(5, 0, 1)
+        across(11)
+        down_pair(5, 0, 1)
+        corner(11)
     else:
         mix_in(0)
         mix_in(1)
@@ -499,32 +529,23 @@
         step(8, 10)
         down_pair(0, 1)
         step(9)
-
-    sides(dn[0])
-    down_send(1, 0, 1)
-    down_pair(1, 0, 1)
-    if role:
-        step(dn[2])
-    sides(dn[1])
-    down_send(2, 0, 1)
-    down_pair(2, 0, 1)
-    across(dn[0])
-    if not role:
-        step(dn[2])
-    finish(0, 0)
-    sides(dn[2])
-    down_send(4, 0, 1)
-    down_pair(4, 0, 1)
-    corner(dn[0])
-    down_send(3, 0, 1)
-    finish(0, 1)
-    across(dn[1])
-    down_pair(3, 0, 1)
-    corner(dn[1])
-    down_send(5, 0, 1)
-    across(dn[2])
-    down_pair(5, 0, 1)
-    corner(dn[2])
+        down_send(1, 0, 1)
+        down_pair(1, 0, 1)
+        down_send(2, 0, 1)
+        down_pair(2, 0, 1)
+        across(8)
+        step(10)
+        down_send(4, 0, 1)
+        down_send(3, 0, 1)
+        down_pair(4, 0, 1)
+        finish(0, 0)
+        across(9)
+        down_pair(3, 0, 1)
+        down_send(5, 0, 1)
+        finish(0, 1)
+        across(10)
+        down_pair(5, 0, 1)
+
     down_send(6, 0, 1)
     finish(1, 0, 1)
     down_pair(6, 0, 1)
@@ -536,7 +557,6 @@
         gated.at[role], RS, BR.at[role], n2.at[pl.ds(0, 4 * half)], RO, ZC,
     )):
         left(ref, w)
-    loaded(out, 9)
 
 
 def paired_local(
@@ -561,11 +581,10 @@
 
     return pl.pallas_call(
         layer_kernel,
-        out_shape=jax.ShapeDtypeStruct((2 * half, width), BF16),
+        out_shape=pltpu.VMEM((2 * half, width), BF16),
         in_specs=[pl.BlockSpec(memory_space=pl.ANY)] * 11,
-        out_specs=pl.BlockSpec(memory_space=pl.ANY),
+        out_specs=pl.BlockSpec(memory_space=pltpu.VMEM),
         scratch_shapes=[
-            vmem(2 * half, width),
             vmem(group, width),
             vmem(group, width),
             vmem(group, width),
@@ -585,7 +604,7 @@
             pltpu.VMEM((1, width), F32),
             pltpu.VMEM(conv_taps.shape, F32),
             pltpu.VMEM((1, width), F32),
-            dma(10),
+            dma(11),
             dma(12),
             *[dma(N_PIECES)] * 4,
             *[dma(2)] * 2,

time: 110 us -> 109 us (level)
  local copies, waits for them, and re-layouts: 2.3 us -> 0.97 us
    unnamed x1, local copies, waits for them, and re-layouts: 2.3 us -> 0.97 us
where the time goes in v4:
time: 109 us; the launch traced here: 108 us
  Pallas kernels  107 us (98%)
    pallas_call x1, Pallas kernels, paired_local(): pl.pallas_call(layer_kernel, out_shape=pltpu.VMEM((2 * half, width), BF16...  107 us

profile of v4, /device:TPU:0, one launch (start us, length us, event | category | flops | bytes accessed | tf_op | source)
XLA Modules:
  0.0 108.5 jit_solution(17405670203010167098)
XLA Ops:
  0.0 107.5 %shard_map.109 = bf16[256,2048]{1,0:T(8,128)(2,1)S(1)} custom-call(bf16[512,2048]{1,0:T(8,128)(2,1)} %refs_0_.1, bf16[512,512]{1,0:T(8,128)(2,1)} %refs_1_.1, bf16[512,512]{1,0:T(8,128)(2,1)} %refs_2_.1, bf16[512,512]{1,0:T(8,128)(2,1)} %refs_3_.1, bf16[512,512]{1,0:T(8,128)(2,1)} %refs_4_.1, bf16[512,1408]{1,0:T(8,128)(2,1)} %refs_5_.1, ...), custom_call_target="tpu_custom_call" | custom-call | tf_op jit(solution)/shard_map/pallas_call | solution.py:582
  107.5 1.0 copy.13

commit v5 on v4

--- a/solution.py
+++ b/solution.py
@@ -44,9 +44,12 @@
     cuts = [i * units // 4 for i in range(4)] + [units]
     if role:
         cuts = [(u * units + 6) // 7 for u in (0, 1, 3, 5, 6)] + [units]
-    pieces += [(2, 0, rows_d, 2 * LANES * a, 2 * LANES * (b - a), 0.32) for a, b in zip(cuts, cuts[1:])]
-    down = (0, n_down // 2, 3 * n_down // 4, n_down)
-    for a, b, share in zip(down, down[1:], (0, 0.25, 0.2)):
+    pieces += [
+        (2, 0, rows_d, 2 * LANES * a, 2 * LANES * (b - a), share)
+        for a, b, share in zip(cuts, cuts[1:], (0.32, 0.32, 0.32, 0.32, 0.32))
+    ]
+    down = (0, n_down // 4, n_down // 2, n_down)
+    for a, b, share in zip(down, down[1:], (0.4, 0.4, 0)):
         pieces.append((3, 0, hid, a, b - a, share))
     return pieces + head[2:]
 
@@ -451,40 +454,40 @@
         across(8)
         arrived(6)
         ffn_rows(6, 0)
+        step(9)
         ffn_rows(6, 1)
         arrived(7)
         ffn_rows(7, 0)
         arrived(8)
         ffn_rows(8, 0)
+        step(10)
         down_send(0, 0)
         ffn_rows(7, 1)
         ffn_rows(8, 1)
         down_pair(0, 0)
         down_send(0, 1)
-        step(9)
         sides(9)
         down_send(1, 0, 1)
         down_pair(0, 1)
         down_pair(1, 0, 1)
-        step(10)
-        finish(0, 0)
-        step(11)
         sides(10)
         down_send(2, 0, 1)
-        finish(0, 1)
+        step(11)
         down_pair(2, 0, 1)
-        sides(11)
         down_send(4, 0, 1)
         across(9)
-        down_send(3, 0, 1)
         down_pair(4, 0, 1)
         across(10)
-        down_pair(3, 0, 1)
+        finish(0, 0)
+        finish(0, 1)
+        corner(9)
+        down_send(3, 0, 1)
         corner(10)
         down_send(5, 0, 1)
+        down_pair(3, 0, 1)
         across(11)
+        down_send(6, 0, 1)
         down_pair(5, 0, 1)
-        corner(11)
     else:
         mix_in(0)
         mix_in(1)
@@ -530,23 +533,23 @@
         down_pair(0, 1)
         step(9)
         down_send(1, 0, 1)
+        down_send(2, 0, 1)
         down_pair(1, 0, 1)
-        down_send(2, 0, 1)
         down_pair(2, 0, 1)
-        across(8)
+        finish(0, 0)
         step(10)
         down_send(4, 0, 1)
+        across(8)
+        across(9)
         down_send(3, 0, 1)
+        down_send(5, 0, 1)
         down_pair(4, 0, 1)
-        finish(0, 0)
-        across(9)
         down_pair(3, 0, 1)
-        down_send(5, 0, 1)
+        down_pair(5, 0, 1)
         finish(0, 1)
         across(10)
-        down_pair(5, 0, 1)
-
-    down_send(6, 0, 1)
+        down_send(6, 0, 1)
+
     finish(1, 0, 1)
     down_pair(6, 0, 1)
     for k in (2, 4, 3, 5, 6):

time: 109 us -> 107 us (0.982)
    pallas_call x1, Pallas kernels: 107 us -> 106 us  [paired_local(): pl.pallas_call(layer_kernel, out_shape=pltpu.VMEM((2 * half, width), BF16...]
where the time goes in v5:
time: 107 us
  Pallas kernels  106 us (99%)
    pallas_call x1, Pallas kernels, paired_local(): pl.pallas_call(layer_kernel, out_shape=pltpu.VMEM((2 * half, width), BF16...  106 us

profile of v5, /device:TPU:0, one launch (start us, length us, event | category | flops | bytes accessed | tf_op | source)
XLA Modules:
  0.0 106.6 jit_solution(8824392520120443905)
XLA Ops:
  0.0 105.6 %shard_map.109 = bf16[256,2048]{1,0:T(8,128)(2,1)S(1)} custom-call(bf16[512,2048]{1,0:T(8,128)(2,1)} %refs_0_.1, bf16[512,512]{1,0:T(8,128)(2,1)} %refs_1_.1, bf16[512,512]{1,0:T(8,128)(2,1)} %refs_2_.1, bf16[512,512]{1,0:T(8,128)(2,1)} %refs_3_.1, bf16[512,512]{1,0:T(8,128)(2,1)} %refs_4_.1, bf16[512,1408]{1,0:T(8,128)(2,1)} %refs_5_.1, ...), custom_call_target="tpu_custom_call" | custom-call | tf_op jit(solution)/shard_map/pallas_call | solution.py:585
  105.6 1.0 copy.13

commit v6 on v5

--- a/solution.py
+++ b/solution.py
@@ -46,10 +46,10 @@
         cuts = [(u * units + 6) // 7 for u in (0, 1, 3, 5, 6)] + [units]
     pieces += [
         (2, 0, rows_d, 2 * LANES * a, 2 * LANES * (b - a), share)
-        for a, b, share in zip(cuts, cuts[1:], (0.32, 0.32, 0.32, 0.32, 0.32))
+        for a, b, share in zip(cuts, cuts[1:], (0.32, 0.32, 0.32, 0.25, 0.25))
     ]
     down = (0, n_down // 4, n_down // 2, n_down)
-    for a, b, share in zip(down, down[1:], (0.4, 0.4, 0)):
+    for a, b, share in zip(down, down[1:], (0.45, 0.45, 0)):
         pieces.append((3, 0, hid, a, b - a, share))
     return pieces + head[2:]
 
@@ -130,7 +130,7 @@
     w_rows = [pl.ds(a, b - a) for a, b in zip(starts, starts[1:])]
     for k in range(len(w_rows)):
         for i, w in enumerate((wb, wc, wi)):
-            load(w.at[w_rows[k], chan], WA.at[f, w_rows[k], pl.ds(i * ch, ch)], (0, 1, 10)[k])
+            load(w.at[w_rows[k], chan], WA.at[f, w_rows[k], pl.ds(i * ch, ch)], (0, 1, 9)[k])
     for h in range(2):
         for core in range(2):
             load(tokens.at[pl.ds((2 * core + h) * half, half)], tok.at[part(2 * h + p, core)], 2)
@@ -232,7 +232,7 @@
         corner(*ks)
 
     for k in range(len(w_rows)):
-        loaded(WA.at[f, w_rows[k]], (0, 1, 10)[k])
+        loaded(WA.at[f, w_rows[k]], (0, 1, 9)[k])
         send((0, 1, 12)[k])
     loaded(tok.at[pl.ds(0, 4 * half)], 2)
     for i, (_, dst) in enumerate(small):
@@ -446,25 +446,25 @@
         ffn_rows(5, 0)
         stream_chunk(2)
         step(8, 9, 10, 11)
+        stream_chunk(3)
         across(7)
-        stream_chunk(3)
         later(2, 3)
         ffn_rows(4, 1)
+        across(8)
         ffn_rows(5, 1)
-        across(8)
         arrived(6)
         ffn_rows(6, 0)
         step(9)
-        ffn_rows(6, 1)
         arrived(7)
         ffn_rows(7, 0)
         arrived(8)
         ffn_rows(8, 0)
+        down_send(0, 0)
         step(10)
-        down_send(0, 0)
+        ffn_rows(6, 1)
+        down_pair(0, 0)
         ffn_rows(7, 1)
         ffn_rows(8, 1)
-        down_pair(0, 0)
         down_send(0, 1)
         sides(9)
         down_send(1, 0, 1)
@@ -607,12 +607,12 @@
             pltpu.VMEM((1, width), F32),
             pltpu.VMEM(conv_taps.shape, F32),
             pltpu.VMEM((1, width), F32),
-            dma(11),
+            dma(10),
             dma(12),
             *[dma(N_PIECES)] * 4,
             *[dma(2)] * 2,
             *[dma(N_CHUNKS)] * 4,
-            *[dma(14)] * 2,
+            *[dma(8)] * 2,
         ],
         compiler_params=pltpu.CompilerParams(
             collective_id=0, has_side_effects=True, vmem_limit_bytes=60 * 2**20

time: 107 us -> 106 us (level)
  no operation moved by 1% of the time
where the time goes in v6:
time: 106 us
  Pallas kernels  105 us (99%)
    pallas_call x1, Pallas kernels, paired_local(): pl.pallas_call(layer_kernel, out_shape=pltpu.VMEM((2 * half, width), BF16...  105 us

profile of v6, /device:TPU:0, one launch (start us, length us, event | category | flops | bytes accessed | tf_op | source)
XLA Modules:
  0.0 106.1 jit_solution(6764469060811708982)
XLA Ops:
  0.0 105.2 %shard_map.109 = bf16[256,2048]{1,0:T(8,128)(2,1)S(1)} custom-call(bf16[512,2048]{1,0:T(8,128)(2,1)} %refs_0_.1, bf16[512,512]{1,0:T(8,128)(2,1)} %refs_1_.1, bf16[512,512]{1,0:T(8,128)(2,1)} %refs_2_.1, bf16[512,512]{1,0:T(8,128)(2,1)} %refs_3_.1, bf16[512,512]{1,0:T(8,128)(2,1)} %refs_4_.1, bf16[512,1408]{1,0:T(8,128)(2,1)} %refs_5_.1, ...), custom_call_target="tpu_custom_call" | custom-call | tf_op jit(solution)/shard_map/pallas_call | solution.py:585
  105.2 1.0 copy.13

commit v7 on v6

--- a/solution.py
+++ b/solution.py
@@ -38,7 +38,7 @@
 
 def weight_pieces(role, rows_d, n_conv, mix_rows, n_mix, units, hid, n_down):
     starts = head_rows(role, rows_d)
-    head = [(0, a, b - a, 0, n_conv, 0.375) for a, b in zip(starts, starts[1:])]
+    head = [(0, a, b - a, 0, n_conv, 0.42) for a, b in zip(starts, starts[1:])]
     pieces = head[:2]
     pieces += [(1, i * mix_rows // 2, mix_rows // 2, 0, n_mix, 0.375) for i in range(2)]
     cuts = [i * units // 4 for i in range(4)] + [units]
@@ -467,8 +467,8 @@
         ffn_rows(8, 1)
         down_send(0, 1)
         sides(9)
+        down_pair(0, 1)
         down_send(1, 0, 1)
-        down_pair(0, 1)
         down_pair(1, 0, 1)
         sides(10)
         down_send(2, 0, 1)

time: 106 us -> 105 us (level)
  no operation moved by 1% of the time
where the time goes in v7:
time: 105 us
  Pallas kernels  104 us (99%)
    pallas_call x1, Pallas kernels, paired_local(): pl.pallas_call(layer_kernel, out_shape=pltpu.VMEM((2 * half, width), BF16...  104 us

profile of v7, /device:TPU:0, one launch (start us, length us, event | category | flops | bytes accessed | tf_op | source)
XLA Modules:
  0.0 105.4 jit_solution(4859406070357956658)
XLA Ops:
  0.0 104.4 %shard_map.109 = bf16[256,2048]{1,0:T(8,128)(2,1)S(1)} custom-call(bf16[512,2048]{1,0:T(8,128)(2,1)} %refs_0_.1, bf16[512,512]{1,0:T(8,128)(2,1)} %refs_1_.1, bf16[512,512]{1,0:T(8,128)(2,1)} %refs_2_.1, bf16[512,512]{1,0:T(8,128)(2,1)} %refs_3_.1, bf16[512,512]{1,0:T(8,128)(2,1)} %refs_4_.1, bf16[512,1408]{1,0:T(8,128)(2,1)} %refs_5_.1, ...), custom_call_target="tpu_custom_call" | custom-call | tf_op jit(solution)/shard_map/pallas_call | solution.py:585
  104.4 1.0 copy.13
